TPU v7x, 512 devices: a whole 4x4x16 slice. The times are simulated.
512 devices in a mesh: ep: 32 (over z, core), tp: 16 (over y, x).
Axes of the slice: x: 4, y: 4, z: 16, core: 2. Of those that a mesh axis runs over, the one named last changes fastest.
Arguments:
- query_maps: bfloat16 [4096, 16, 128], P('ep', 'tp'), may hold values from -6 to 6
- key_maps: bfloat16 [4096, 16, 128], P('ep', 'tp'), may hold values from -6 to 6
- value_rows: bfloat16 [4096, 16, 128], P('ep', 'tp'), may hold values from -6 to 6
- head_lambda: float32 [16], P('tp'), may hold values from 0.3 to 0.8
- head_gain: float32 [128], replicated, may hold values from 0.1 to 1.9
- out_weight: bfloat16 [2048, 2048], P('tp'), may hold values from -0.125 to 0.125
- token_rows: bfloat16 [4096, 2048], P('ep'), may hold values from -36 to 36
- norm_gain: float32 [2048], replicated, may hold values from 0.1 to 1.9
- expert_ids: int32 [4096, 4], P('ep'), may hold values from 0 to 31, all different within a row; in each aligned block of 128 rows (0 to 127, 128 to 255, ...) at most 20 rows name the same one
- route_weights: float32 [4096, 4], P('ep'), may hold values from 0.1 to 0.5
- gate_weight: bfloat16 [32, 2048, 4096], P('ep', None, 'tp'), may hold values from -0.82864076 to 0.82864076
- up_weight: bfloat16 [32, 2048, 4096], P('ep', None, 'tp'), may hold values from -0.82864076 to 0.82864076
- down_weight: bfloat16 [32, 4096, 2048], P('ep', 'tp'), may hold values from -0.03125 to 0.03125
Outputs:
- mixed_rows: bfloat16 [4096, 2048], P(('ep', 'tp'))
- mixed_experts: bfloat16 [4096, 2048], P('ep', 'tp')
Inputs may be any that keep to these rules, and one draw needn't show every extreme that they name: `expert_ids`: each row names 4 different experts. Among the rows of one index of ep no expert is named more than 20 times, and in every draw some expert is named exactly 20 times there.
All inputs are finite; a program needn't handle non-finite values.
Results may differ from a plain program's by a relative error of at most 0.015.
Values may be sent and summed in bfloat16 or wider, within the bound.
A program may use at most 64 MiB of HBM per device.

v0:
```python
import jax
import jax.numpy as jnp
from jax import lax
from jax.sharding import PartitionSpec as P

NORM_EPS = 1e-05
CLAMP_LIMIT = 7.0
GATE_SLOPE = 1.702


def sent_together(arrays, axis, dim, along):
    ends, at = ([], 0)
    for a in arrays[:-1]:
        at += a.shape[along]
        ends.append(at)
    both = jnp.concatenate(arrays, axis=along)
    return tuple(jnp.split(lax.all_gather(both, axis, axis=dim, tiled=True), ends, axis=along))


def in_blocks(array, dim, length):
    lengths = array.shape
    tiles = array.reshape(*lengths[:dim], length, lengths[dim] // length, *lengths[dim + 1 :])
    return jnp.moveaxis(tiles, dim, 0)


def sum_at_owner(array, axis, dim):
    tiles = in_blocks(array, dim, lax.axis_size(axis))
    arrived = lax.all_to_all(tiles, axis, split_axis=0, concat_axis=0, tiled=True)
    return arrived.astype(jnp.float32).sum(axis=0)


def sent_to_all(array, axis):
    length = lax.axis_size(axis)
    return lax.all_to_all(
        jnp.broadcast_to(array[None], (length, *array.shape)), axis, 0, 0, tiled=True
    )


def laid_out(tiles, dim):
    tiles = jnp.moveaxis(tiles, 0, dim)
    lengths = tiles.shape
    return tiles.reshape(*lengths[:dim], lengths[dim] * lengths[dim + 1], *lengths[dim + 2 :])


def collect(array, axis, dim):
    tiles = sent_to_all(array, axis)
    return laid_out(tiles, dim)


def fold_rows(queries, positions, running, key_block, value_block, offset, head_width, score_scale):
    key_pos = jnp.arange(key_block.shape[0], dtype=jnp.int32)
    causal = key_pos[None, None, :] <= positions[None, :, None]

    def update(running_state):
        fresh = []
        for map_index in range(2):
            row_max, denominator, numerator = running_state[map_index]
            col_low = map_index * head_width
            col_high = col_low + head_width
            scores = (
                jnp.einsum(
                    "qhd,khd->hqk",
                    queries[:, :, col_low:col_high],
                    key_block[:, :, col_low:col_high],
                    preferred_element_type=jnp.float32,
                )
                * score_scale
            )
            scores = jnp.where(causal, scores, -jnp.inf)
            new_max = jnp.maximum(row_max, jnp.max(scores, axis=-1))
            exp_terms = jnp.exp(scores - new_max[:, :, None])
            denominator = jnp.sum(exp_terms, axis=-1)
            numerator = jnp.einsum(
                "hqk,khd->qhd",
                exp_terms.astype(jnp.bfloat16),
                value_block,
                preferred_element_type=jnp.float32,
            )
            fresh.append((new_max, denominator, numerator))
        return tuple(fresh)

    def unchanged(running_state):
        return running_state

    return lax.cond(offset <= positions[positions.shape[0] - 1], update, unchanged, running)


def finish_rows(state, head_lambda, head_gain):
    first_map, second_map = state
    attended = first_map[2] / jnp.transpose(first_map[1])[:, :, None] - head_lambda[
        None, :, None
    ] * (second_map[2] / jnp.transpose(second_map[1])[:, :, None])
    mean_sq = jnp.mean(attended * attended, axis=-1, keepdims=True)
    return (attended * lax.rsqrt(mean_sq + NORM_EPS) * head_gain).astype(jnp.bfloat16)


def mixer_half(query_maps, key_maps, value_rows, head_lambda, head_gain, out_weight):
    local_rows = query_maps.shape[0]
    local_heads = query_maps.shape[1]
    head_width = query_maps.shape[2] // 2
    score_scale = head_width ** (-0.5)
    half_rows = local_rows // 2
    ep_index = lax.axis_index("ep")
    early_queries = query_maps[:half_rows]
    late_queries = query_maps[half_rows:]
    early_pos = ep_index * local_rows + jnp.arange(half_rows, dtype=jnp.int32)
    late_pos = ep_index * local_rows + half_rows + jnp.arange(half_rows, dtype=jnp.int32)
    one_map = (
        jnp.full((local_heads, half_rows), -1e30, jnp.float32),
        jnp.zeros((local_heads, half_rows), jnp.float32),
        jnp.zeros((half_rows, local_heads, 2 * head_width), jnp.float32),
    )
    offset = jnp.int32(0)
    key_block, value_block = sent_together((key_maps, value_rows), "ep", 0, 1)
    early_state = fold_rows(
        early_queries,
        early_pos,
        (one_map, one_map),
        key_block,
        value_block,
        offset,
        head_width,
        score_scale,
    )
    late_state = fold_rows(
        late_queries,
        late_pos,
        (one_map, one_map),
        key_block,
        value_block,
        offset,
        head_width,
        score_scale,
    )
    early_state, late_state = (early_state, late_state)
    early_rows = finish_rows(early_state, head_lambda, head_gain)
    late_rows = finish_rows(late_state, head_lambda, head_gain)
    head_rows = jnp.concatenate([early_rows, late_rows], axis=0).reshape(
        local_rows, local_heads * 2 * head_width
    )
    product = jnp.dot(head_rows, out_weight, preferred_element_type=jnp.float32)
    summed = sum_at_owner(
        lax.optimization_barrier(product.astype(jnp.bfloat16))
        .astype(jnp.float32)
        .astype(jnp.bfloat16),
        "tp",
        0,
    )
    return summed.astype(jnp.bfloat16)


def complete_experts(gate_pre, up_pre, down_matrix):
    gated = jnp.minimum(gate_pre, CLAMP_LIMIT)
    clipped = jnp.clip(up_pre, -CLAMP_LIMIT, CLAMP_LIMIT)
    active = ((clipped + 1.0) * gated * jax.nn.sigmoid(GATE_SLOPE * gated)).astype(jnp.bfloat16)
    partial_value = jnp.einsum(
        "scf,fd->scd", active, down_matrix, preferred_element_type=jnp.float32
    )
    partial_value = lax.optimization_barrier(partial_value.astype(jnp.bfloat16)).astype(jnp.float32)
    summed = sum_at_owner(partial_value.astype(jnp.bfloat16), "tp", 2)
    return lax.all_to_all(
        summed.astype(jnp.bfloat16), "ep", split_axis=0, concat_axis=0, tiled=True
    )


def expert_half(
    token_rows, norm_gain, expert_ids, route_weights, gate_weight, up_weight, down_weight
):
    local_rows, model_width = token_rows.shape
    route_count = expert_ids.shape[1]
    expert_count = lax.axis_size("ep")
    capacity = 5 * local_rows * route_count // (4 * expert_count)
    gate_matrix = gate_weight[0]
    up_matrix = up_weight[0]
    down_matrix = down_weight[0]
    rows_float = token_rows.astype(jnp.float32)
    mean_sq = jnp.mean(rows_float * rows_float, axis=-1, keepdims=True)
    normed = (rows_float * lax.rsqrt(mean_sq + NORM_EPS) * norm_gain).astype(jnp.bfloat16)
    flat_ids = expert_ids.reshape(-1)
    onehot = (flat_ids[:, None] == jnp.arange(expert_count, dtype=jnp.int32)[None, :]).astype(
        jnp.int32
    )
    rank_before = jnp.cumsum(onehot, axis=0) - onehot
    slot_of = jnp.sum(rank_before * onehot, axis=1)
    target = flat_ids * capacity + slot_of
    token_of = jnp.arange(local_rows * route_count, dtype=jnp.int32) // route_count
    slot_table = (
        jnp.full((expert_count * capacity,), local_rows, jnp.int32).at[target].set(token_of)
    )
    padded = jnp.concatenate([normed, jnp.zeros((1, model_width), jnp.bfloat16)], axis=0)
    outgoing = padded[slot_table].reshape(expert_count, capacity, model_width)
    feature_width = model_width // lax.axis_size("tp")
    outgoing_part = lax.dynamic_slice_in_dim(
        outgoing, lax.axis_index("tp") * feature_width, feature_width, 2
    )
    feature_block = collect(
        lax.all_to_all(outgoing_part, "ep", split_axis=0, concat_axis=0, tiled=True), "tp", 2
    )
    gate_sum = jnp.einsum(
        "scd,df->scf", feature_block, gate_matrix, preferred_element_type=jnp.float32
    )
    up_sum = jnp.einsum("scd,df->scf", feature_block, up_matrix, preferred_element_type=jnp.float32)
    returned = complete_experts(gate_sum, up_sum, down_matrix)
    result_width = returned.shape[2]
    picked = returned.reshape(expert_count * capacity, result_width)[target].astype(jnp.float32)
    weighted = picked * route_weights.reshape(-1)[:, None]
    combined = jnp.sum(weighted.reshape(local_rows, route_count, result_width), axis=1)
    return combined.astype(jnp.bfloat16)


def body(
    query_maps,
    key_maps,
    value_rows,
    head_lambda,
    head_gain,
    out_weight,
    token_rows,
    norm_gain,
    expert_ids,
    route_weights,
    gate_weight,
    up_weight,
    down_weight,
):
    mixed_rows = mixer_half(query_maps, key_maps, value_rows, head_lambda, head_gain, out_weight)
    mixed_experts = expert_half(
        token_rows, norm_gain, expert_ids, route_weights, gate_weight, up_weight, down_weight
    )
    return (mixed_rows, mixed_experts)


def solution(mesh):
    placed = (
        P("ep", "tp", None),
        P("ep", "tp", None),
        P("ep", "tp", None),
        P("tp"),
        P(),
        P("tp", None),
        P("ep", None),
        P(),
        P("ep", None),
        P("ep", None),
        P("ep", None, "tp"),
        P("ep", None, "tp"),
        P("ep", "tp", None),
    )
    return jax.shard_map(
        body,
        mesh=mesh,
        in_specs=placed,
        out_specs=(P(("ep", "tp"), None), P("ep", "tp")),
        check_vma=False,
    )
```

profile of v0, /device:TPU:1, one launch (start us, length us, event | category | flops | bytes accessed | tf_op | source)
XLA Modules:
  0.0 208.6 jit_solution(8947306529190692896)
XLA Ops:
  7.2 0.8 broadcast_multiply_fusion
  8.0 0.8 copy.44
  9.0 1.2 fusion.66
  10.5 1.2 reduce-window.6
  12.0 2.4 %scatter_custom_fusion = s32[640]{0:T(1024)S(1)} fusion(s32[512]{0:T(512)S(1)} %bitcast.195, s32[512]{0:T(512)S(1)} %add_select_fusion, s32[]{:T(128)} %constant.42.clone.1), kind=kCustom, calls=%fused_computation.126 | custom fusion | bytes 2564 | tf_op jit(solution)/shard_map/scatter | solution.py:188
  14.5 1.2 fusion.68
  15.8 4.1 %gather_fusion = bf16[640,2048]{1,0:T(8,128)(2,1)} fusion(bf16[129,2048]{1,0:T(8,128)(2,1)S(1)} %concatenate.11, s32[1024]{0:T(1024)S(1)} %pad_clamp_fusion.1), kind=kCustom, calls=%fused_computation | custom fusion | bytes 5245440 | tf_op jit(solution)/shard_map/gather | solution.py:191
  19.9 5.2 %reshape.273 = bf16[32,20,2048]{2,1,0:T(8,128)(2,1)} reshape(bf16[640,2048]{1,0:T(8,128)(2,1)} %gather_fusion) | data formatting | bytes 5242880 | tf_op jit(solution)/shard_map/reshape | solution.py:191
  25.1 1.6 constant_dynamic-slice_fusion
  26.7 16.7 %all-to-all-start.1 = ((bf16[32,20,128]{2,1,0:T(8,128)(2,1)}), bf16[32,20,128]{2,1,0:T(8,128)(2,1)S(1)}, u32[]{:S(2)}, u32[]{:S(2)}) async-start(bf16[32,20,128]{2,1,0:T(8,128)(2,1)} %constant_dynamic-slice_fusion), calls=%async_computation.1 | async-start | bytes 393216 | tf_op jit(solution)/shard_map/all_to_all | solution.py:197
  43.5 0.6 pad_maximum_fusion
  44.2 18.0 %all-to-all-done.1 = bf16[32,20,128]{2,1,0:T(8,128)(2,1)S(1)} async-done(((bf16[32,20,128]{2,1,0:T(8,128)(2,1)}), bf16[32,20,128]{2,1,0:T(8,128)(2,1)S(1)}, u32[]{:S(2)}, u32[]{:S(2)}) %all-to-all-start.1) | async-done | bytes 163872 | tf_op jit(solution)/shard_map/all_to_all | solution.py:197
  62.3 0.5 broadcast_in_dim.39
  62.8 39.4 %all_to_all.25 = bf16[16,32,20,128]{3,1,2,0:T(8,128)(2,1)S(1)} all-to-all(bf16[16,32,20,128]{3,1,2,0:T(8,128)(2,1)S(1)} %broadcast_in_dim.39), channel_id=1, replica_groups=mesh['ep'=32,'tp'=16] {'tp'}, dimensions={0} | all-to-all | bytes 5242880 | tf_op jit(solution)/shard_map/all_to_all | solution.py:34
  102.2 1.5 copy-done.3
  103.7 0.8 fusion.49
  104.9 6.1 %convolution_convert_fusion = bf16[32,20,2048]{2,0,1:T(8,128)(2,1)} fusion(f32[32,20,256]{2,0,1:T(8,128)S(1)} %fusion.49, bf16[1,256,2048]{2,1,0:T(8,128)(2,1)S(1)} %copy-done, bf16[1,2048,256]{2,1,0:T(8,128)(2,1)S(1)} %copy-done.10, bf16[16,32,20,128]{3,1,2,0:T(8,128)(2,1)} %copy-done.3), kind=kOutput, calls=%fused_computation.63 | convolution fusion | flops 1344962560 | bytes 7995392 | tf_op jit(solution)/shard_map/scf,fd->scd/dot_general | solution.py:156
  111.0 3.9 %bitcast_bitcast_fusion = bf16[16,32,20,128]{3,1,2,0:T(8,128)(2,1)} fusion(bf16[32,20,2048]{2,0,1:T(8,128)(2,1)} %convolution_convert_fusion), kind=kLoop, calls=%fused_computation.68 | loop fusion | bytes 5242880 | tf_op jit(solution)/shard_map/transpose | solution.py:23
  114.9 4.4 %all-to-all-start.3 = ((bf16[16,32,20,128]{3,1,2,0:T(8,128)(2,1)}), bf16[16,32,20,128]{3,1,2,0:T(8,128)(2,1)}, u32[]{:S(2)}, u32[]{:S(2)}) async-start(bf16[16,32,20,128]{3,1,2,0:T(8,128)(2,1)} %bitcast_bitcast_fusion), calls=%async_computation.3 | async-start | bytes 5242880 | tf_op jit(solution)/shard_map/all_to_all | solution.py:28
  119.4 0.7 slice.45
  121.4 0.6 slice.44
  122.6 1.7 fusion.103
  124.4 0.6 iota.36
  125.0 1.1 le.45
  126.1 5.0 %conditional.3 = (f32[1,64]{1,0:T(1,128)S(1)}, f32[64,1,128]{2,0,1:T(8,128)S(1)}, f32[1,64]{1,0:T(1,128)S(1)}, f32[64,1,128]{2,0,1:T(8,128)S(1)}) conditional(s32[]{:T(128)} %bitcast.40, () %tuple.26, (s32[]{:T(128)}, s32[1,64,1]{1,2,0:T(1,128)S(1)}, s32[1,64,4096]{2,1,0:T(8,128)S(1)}, bf16[128,1,128]{2,0,1:T(8,128)(2,1)S(1)}, ...), branch_computations={%region_7.8_spmd, %region_8.13_spmd} | conditional | flops 205258688 | bytes 17665856 | solution.py:85
  126.3 1.3 copy.42
  127.6 1.5 fusion.101
  129.9 0.5 fusion.102
  131.1 8.8 %conditional.2 = (f32[1,64]{1,0:T(1,128)}, f32[64,1,128]{2,0,1:T(8,128)S(1)}, f32[1,64]{1,0:T(1,128)}, f32[64,1,128]{2,0,1:T(8,128)}) conditional(s32[]{:T(128)} %bitcast.36, () %tuple.24, (s32[]{:T(128)}, s32[1,64,1]{1,2,0:T(1,128)}, s32[1,64,4096]{2,1,0:T(8,128)}, bf16[128,1,128]{2,0,1:T(8,128)(2,1)S(1)}, bf16[4096,1,128]{2,0,1:T(8,128)(2,1)S(1)}, ...), branch_computations={%region_0.0_spmd, %region_1.6_spmd} | conditional | flops 205258688 | bytes 17665856 | solution.py:85
  131.3 0.7 add_bitcast_fusion
  132.0 1.4 broadcast_compare_fusion
  133.4 1.3 copy.41
  134.8 1.5 fusion.99
  136.3 0.9 fusion.7
  138.0 0.9 fusion.9
  138.9 1.0 convolution_bitcast_fusion
  139.9 1.0 multiply_reduce_fusion
  141.0 2.1 %convolution_convert_fusion.1 = bf16[128,2048]{1,0:T(8,128)(2,1)} fusion(bf16[128,2048]{1,0:T(8,128)(2,1)} %param.22, bf16[64,1,128]{2,0,1:T(8,128)(2,1)S(1)} %get-tuple-element.129, bf16[64,1,128]{2,0,1:T(8,128)(2,1)S(1)} %get-tuple-element.128), kind=kOutput, calls=%fused_computation.69 | convolution fusion | flops 67436544 | bytes 1081344 | tf_op jit(solution)/shard_map/dot_general | solution.py:141
  143.1 10.3 %all-to-all-done.3 = bf16[16,32,20,128]{3,1,2,0:T(8,128)(2,1)} async-done(((bf16[16,32,20,128]{3,1,2,0:T(8,128)(2,1)}), bf16[16,32,20,128]{3,1,2,0:T(8,128)(2,1)}, u32[]{:S(2)}, u32[]{:S(2)}) %all-to-all-start.3) | async-done | bytes 2621472 | tf_op jit(solution)/shard_map/all_to_all | solution.py:28
  153.5 6.1 %all-to-all-start = ((bf16[16,8,2048]{2,1,0:T(8,128)(2,1)}), bf16[16,8,2048]{2,1,0:T(8,128)(2,1)S(1)}, u32[]{:S(2)}, u32[]{:S(2)}) async-start(bf16[16,8,2048]{2,1,0:T(8,128)(2,1)} %bitcast.44), calls=%async_computation | async-start | bytes 1048576 | tf_op jit(solution)/shard_map/all_to_all | solution.py:28
  159.6 2.1 %reduce_sum.121 = bf16[32,20,128]{2,0,1:T(8,128)(2,1)S(1)} reduce(bf16[16,32,20,128]{3,1,2,0:T(8,128)(2,1)} %all-to-all-done.3, bf16[]{:T(256)} %constant.81.clone.1), dimensions={0}, to_apply=%region_20.21 | reduce | flops 1228800 | bytes 2785282 | tf_op jit(solution)/shard_map/reduce_sum | solution.py:29
  161.7 0.7 copy.51
  162.4 7.4 %all-to-all-done = bf16[16,8,2048]{2,1,0:T(8,128)(2,1)S(1)} async-done(((bf16[16,8,2048]{2,1,0:T(8,128)(2,1)}), bf16[16,8,2048]{2,1,0:T(8,128)(2,1)S(1)}, u32[]{:S(2)}, u32[]{:S(2)}) %all-to-all-start) | async-done | bytes 524320 | tf_op jit(solution)/shard_map/all_to_all | solution.py:28
  169.8 10.9 %all-to-all-start.4 = ((bf16[32,20,128]{2,1,0:T(8,128)(2,1)}), bf16[32,20,128]{2,1,0:T(8,128)(2,1)S(1)}, u32[]{:S(2)}, u32[]{:S(2)}) async-start(bf16[32,20,128]{2,1,0:T(8,128)(2,1)} %copy.51), calls=%async_computation.4 | async-start | bytes 393216 | tf_op jit(solution)/shard_map/all_to_all | solution.py:161
  180.8 0.7 reduce_sum.117
  181.5 18.0 %all-to-all-done.4 = bf16[32,20,128]{2,1,0:T(8,128)(2,1)S(1)} async-done(((bf16[32,20,128]{2,1,0:T(8,128)(2,1)}), bf16[32,20,128]{2,1,0:T(8,128)(2,1)S(1)}, u32[]{:S(2)}, u32[]{:S(2)}) %all-to-all-start.4) | async-done | bytes 163872 | tf_op jit(solution)/shard_map/all_to_all | solution.py:161
  199.5 1.3 gather_fusion.1
  200.9 0.9 fusion.82
  (62 shorter events, 4.2 us)
Async XLA Ops:
  7.2 97.4 %copy-start = (bf16[1,256,2048]{2,1,0:T(8,128)(2,1)S(1)}, bf16[1,256,2048]{2,1,0:T(8,128)(2,1)}, u32[]{:S(2)}) copy-start(bf16[1,256,2048]{2,1,0:T(8,128)(2,1)} %param.29) | copy-start | bytes 3145732
  19.9 23.6 %copy-start.5 = (bf16[128,1,128]{2,0,1:T(8,128)(2,1)S(1)}, bf16[128,1,128]{2,0,1:T(8,128)(2,1)}, u32[]{:S(2)}) copy-start(bf16[128,1,128]{2,0,1:T(8,128)(2,1)} %param.19) | copy-start | bytes 98308
  19.9 23.6 %copy-start.6 = (bf16[128,1,128]{2,0,1:T(8,128)(2,1)S(1)}, bf16[128,1,128]{2,0,1:T(8,128)(2,1)}, u32[]{:S(2)}) copy-start(bf16[128,1,128]{2,0,1:T(8,128)(2,1)} %param.18) | copy-start | bytes 98308
  26.7 35.5 %all-to-all-start.1 = ((bf16[32,20,128]{2,1,0:T(8,128)(2,1)}), bf16[32,20,128]{2,1,0:T(8,128)(2,1)S(1)}, u32[]{:S(2)}, u32[]{:S(2)}) async-start(bf16[32,20,128]{2,1,0:T(8,128)(2,1)} %constant_dynamic-slice_fusion), calls=%async_computation.1 | async-start | bytes 393216 | tf_op jit(solution)/shard_map/all_to_all | solution.py:197
  43.4 79.2 %all-gather.2.cloned.1.call-start = ((), (), s32[]{:S(2)}) async-start(), calls=%async_computation.5 | async-start | bytes 2162688 | tf_op jit(solution)/shard_map/all_gather | solution.py:17
  62.8 40.9 %copy-start.9 = (bf16[1,2048,256]{2,1,0:T(8,128)(2,1)S(1)}, bf16[1,2048,256]{2,1,0:T(8,128)(2,1)}, u32[]{:S(2)}) copy-start(bf16[1,2048,256]{2,1,0:T(8,128)(2,1)} %param.27) | copy-start | bytes 3145732
  102.2 1.5 copy-start.3
  103.7 1.2 copy-start.10
  114.9 38.5 %all-to-all-start.3 = ((bf16[16,32,20,128]{3,1,2,0:T(8,128)(2,1)}), bf16[16,32,20,128]{3,1,2,0:T(8,128)(2,1)}, u32[]{:S(2)}, u32[]{:S(2)}) async-start(bf16[16,32,20,128]{3,1,2,0:T(8,128)(2,1)} %bitcast_bitcast_fusion), calls=%async_computation.3 | async-start | bytes 5242880 | tf_op jit(solution)/shard_map/all_to_all | solution.py:28
  122.6 3.5 %copy-start.4 = (bf16[128,1,128]{2,0,1:T(8,128)(2,1)S(1)}, bf16[128,1,128]{2,0,1:T(8,128)(2,1)}, u32[]{:S(2)}) copy-start(bf16[128,1,128]{2,0,1:T(8,128)(2,1)} %param.17) | copy-start | bytes 98308
  127.6 2.3 %copy-start.1 = (bf16[4096,1,128]{0,2,1:T(8,128)(2,1)S(1)}, bf16[4096,1,128]{0,2,1:T(8,128)(2,1)}, u32[]{:S(2)}) copy-start(bf16[4096,1,128]{0,2,1:T(8,128)(2,1)} %copy.42) | copy-start | bytes 3145732 | tf_op jit(solution)/shard_map/cond
  131.1 9.8 %copy-start.8 = (f32[128]{0:T(128)S(1)}, f32[128]{0:T(128)}, u32[]{:S(2)}) copy-start(f32[128]{0:T(128)} %param.21) | copy-start | bytes 1540
  134.8 2.8 %copy-start.2 = (bf16[4096,1,128]{0,2,1:T(8,128)(2,1)S(1)}, bf16[4096,1,128]{0,2,1:T(8,128)(2,1)}, u32[]{:S(2)}) copy-start(bf16[4096,1,128]{0,2,1:T(8,128)(2,1)} %copy.41) | copy-start | bytes 3145732 | tf_op jit(solution)/shard_map/cond
  141.0 39.7 %copy-start.7 = (f32[128,4]{0,1:T(4,128)S(1)}, f32[128,4]{0,1:T(4,128)}, u32[]{:S(2)}) copy-start(f32[128,4]{0,1:T(4,128)} %param.26) | copy-start | bytes 6148
  153.5 16.3 %all-to-all-start = ((bf16[16,8,2048]{2,1,0:T(8,128)(2,1)}), bf16[16,8,2048]{2,1,0:T(8,128)(2,1)S(1)}, u32[]{:S(2)}, u32[]{:S(2)}) async-start(bf16[16,8,2048]{2,1,0:T(8,128)(2,1)} %bitcast.44), calls=%async_computation | async-start | bytes 1048576 | tf_op jit(solution)/shard_map/all_to_all | solution.py:28
  169.8 29.7 %all-to-all-start.4 = ((bf16[32,20,128]{2,1,0:T(8,128)(2,1)}), bf16[32,20,128]{2,1,0:T(8,128)(2,1)S(1)}, u32[]{:S(2)}, u32[]{:S(2)}) async-start(bf16[32,20,128]{2,1,0:T(8,128)(2,1)} %copy.51), calls=%async_computation.4 | async-start | bytes 393216 | tf_op jit(solution)/shard_map/all_to_all | solution.py:161
Sparse Core Ops, SparseCore 0:
  46.4 72.5 all-gather.1
where the time goes:
time: 210 us; the launch traced here: 209 us
  waiting for transfers between devices  53.7 us (26%)
  blocking collectives  39.4 us (19%)
  starting transfers between devices  38.2 us (18%)
  local copies, waits for them, and re-layouts  30.8 us (15%)
  between operations  16.3 us (8%)
  matrix products  15.2 us (7%)
  other arithmetic  14.7 us (7%)
    all_to_all x1, blocking collectives, sent_to_all(): lax.all_to_all(jnp.broadcast_to(array[None], (length, *array.shape)), axi...  39.4 us
    all_to_all x1, waiting for transfers between devices, expert_half(): lax.all_to_all(outgoing_part, 'ep', split_axis=0, concat_axis=0, tiled=True)  18 us
    all_to_all x1, waiting for transfers between devices, complete_experts(): lax.all_to_all(summed.astype(jnp.bfloat16), 'ep', split_axis=0, concat_ax...  18 us
    all_to_all x2, waiting for transfers between devices, sum_at_owner(): lax.all_to_all(tiles, axis, split_axis=0, concat_axis=0, tiled=True)  17.7 us
    all_to_all x1, starting transfers between devices, expert_half(): lax.all_to_all(outgoing_part, 'ep', split_axis=0, concat_axis=0, tiled=True)  16.7 us
    all_to_all x1, starting transfers between devices, complete_experts(): lax.all_to_all(summed.astype(jnp.bfloat16), 'ep', split_axis=0, concat_ax...  10.9 us
    all_to_all x2, starting transfers between devices, sum_at_owner(): lax.all_to_all(tiles, axis, split_axis=0, concat_axis=0, tiled=True)  10.5 us
    dot_general x1, matrix products, complete_experts(): jnp.einsum('scf,fd->scd', active, down_matrix, preferred_element_type=jnp...  6.09 us
  transfers between devices with their start and end apart: 5, of which 4 were waited for; matrix products, arithmetic and copies ran while one was open for 18% of the time, Pallas kernels for 0%

commit v1 on v0

v1 whole, which is shorter than its diff:
```python
import functools

import jax
import jax.numpy as jnp
import numpy as np
from jax import lax
from jax.experimental import pallas as pl
from jax.experimental.pallas import tpu as pltpu
from jax.sharding import PartitionSpec as P

NORM_EPS = 1e-05
CLAMP_LIMIT = 7.0
GATE_SLOPE = 1.702
MESH = pl.DeviceIdType.MESH

EP, TP, SIDE, CHIPS = 32, 16, 4, 16
CAP, SLAB = 20, 24
ROWS, HALF = EP * CAP, EP * CAP // 2
PADDED, PAD_HALF = EP * SLAB, EP * SLAB // 2
D, LANE, TOK, UNITS = 2048, 128, 128, 256
BAND = SIDE * LANE
TILE = 160
F32, BF16 = jnp.float32, jnp.bfloat16
NN = (((1,), (0,)), ((), ()))
NT = (((1,), (1,)), ((), ()))


def mm(a, b, dims=NN):
    return lax.dot_general(a, b, dims, preferred_element_type=F32)


def slot_tables():
    rows = np.arange(PADDED)
    spread = np.zeros((PADDED, LANE), np.float32)
    spread[rows, rows // SLAB] = 1.0
    spread[rows, EP] = -(rows % SLAB)
    pack = np.zeros((HALF, PAD_HALF), np.float32)
    r = np.arange(HALF)
    pack[r, r // CAP * SLAB + r % CAP] = 1.0
    return spread, pack, pack.T.copy()


def kernel(
    qkv_ref, lam_ref, gain_ref, ow_hbm, tok_ref, ngain_ref, ids_ref, wts_ref, spread_ref, pack_ref, unpack_ref,
    gate_hbm, up_hbm, down_hbm,
    rows_ref, experts_ref,
    kv, m_ref, l_ref, acc_ref, psend, prec, xsend, xrec, xall, ypart, rs1a, rs1b, z0, z1, rs2a, rs2b, rsend, rrec,
    ow_ref, gate_ref, up_ref, down_ref,
    local_sem, plus_s, plus_r, minus_s, minus_r, sib_s, sib_r, p_s, p_r, d_s, d_r, ag1_s, ag1_r, ag2_s, ag2_r,
    r1_s, r1_r, r2_s, r2_r, b_s, b_r,
):
    ep = lax.axis_index("ep")
    tp = lax.axis_index("tp")
    z, core = ep // 2, ep % 2
    x, y = tp % SIDE, tp // SIDE
    sib = z * 2 + (1 - core)

    def lanes(block, width=LANE):
        return pl.ds(pl.multiple_of(block * width, width), width)

    def remote(src, dst, ssem, rsem, e, t):
        return pltpu.make_async_remote_copy(
            src_ref=src, dst_ref=dst, send_sem=ssem, recv_sem=rsem, device_id=(e, t), device_id_type=MESH
        )

    def x_peer(j):
        return y * SIDE + (x + j) % SIDE

    def y_peer(j):
        return ((y + j) % SIDE) * SIDE + x

    barrier = pltpu.get_barrier_semaphore()

    def greet_ep(i, carry):
        pl.semaphore_signal(barrier, inc=1, device_id=((ep + i) % EP, tp), device_id_type=MESH)
        return carry

    def greet_tp(i, carry):
        pl.semaphore_signal(barrier, inc=1, device_id=(ep, (tp + i) % TP), device_id_type=MESH)
        return carry

    lax.fori_loop(1, EP, greet_ep, 0)
    lax.fori_loop(1, TP, greet_tp, 0)

    weight_copies = [
        pltpu.make_async_copy(src, dst, local_sem.at[i])
        for i, (src, dst) in enumerate(((gate_hbm, gate_ref), (up_hbm, up_ref), (down_hbm, down_ref), (ow_hbm, ow_ref)))
    ]
    for copy in weight_copies:
        copy.start()

    tokens = tok_ref[...].astype(F32)
    scale = lax.rsqrt(jnp.mean(tokens * tokens, axis=-1, keepdims=True) + NORM_EPS)
    mine = tok_ref[:, lanes(tp)].astype(F32)
    normed = (mine * scale * ngain_ref[:, lanes(tp)]).astype(BF16)
    expert = lax.broadcasted_iota(jnp.int32, (TOK, LANE), 1)
    token = lax.broadcasted_iota(jnp.int32, (TOK, LANE), 0)
    named = jnp.zeros((TOK, LANE), F32)
    weight = jnp.zeros((TOK, LANE), F32)
    for k in range(4):
        hit = ids_ref[:, k : k + 1] == expert
        named = named + jnp.where(hit, 1.0, 0.0)
        weight = weight + jnp.where(hit, wts_ref[:, k : k + 1], 0.0)
    before = jnp.where(expert < token, 1.0, 0.0).astype(BF16)
    rank = mm(before, named.astype(BF16))
    place = jnp.where(named > 0.5, rank, -1.0)
    place = jnp.where(expert < EP, place, jnp.where(expert == EP, 1.0, 0.0))
    spread = spread_ref[...]
    chosen = mm(spread, jnp.transpose(place).astype(BF16))
    chosen = jnp.where(jnp.abs(chosen) < 0.5, 1.0, 0.0).astype(BF16)
    outgoing = mm(chosen, normed).astype(BF16)
    for e in range(EP):
        xsend[e] = outgoing[e * SLAB : (e + 1) * SLAB]
    kv[ep] = qkv_ref[1:3]

    pl.semaphore_wait(barrier, EP - 1 + TP - 1)

    def dispatch(i):
        peer = (ep + i) % EP
        return remote(xsend.at[peer], xrec.at[ep], d_s.at[i], d_r.at[ep], peer, tp)

    def dispatch_order(n):
        off = (n + 1) // 2
        return EP // 2 + off * (1 - 2 * (n % 2))

    def dispatch_all(n, carry):
        dispatch(dispatch_order(n)).start()
        return carry

    lax.fori_loop(0, EP - 1, dispatch_all, 0)

    def plus(d):
        block = 2 * (z - d) + core
        return remote(kv.at[block], kv.at[block], plus_s.at[d], plus_r.at[d + 1], ep + 2, tp)

    def plus_in(d):
        block = 2 * (z - d) + core
        return remote(kv.at[block], kv.at[block], plus_s.at[d - 1], plus_r.at[d], ep + 2, tp)

    def minus(d):
        block = 2 * ((z + d) % CHIPS) + core
        return remote(kv.at[block], kv.at[block], minus_s.at[d], minus_r.at[d + 1], (ep + EP - 2) % EP, tp)

    def minus_in(d):
        block = 2 * ((z + d) % CHIPS) + core
        return remote(kv.at[block], kv.at[block], minus_s.at[d - 1], minus_r.at[d], (ep + EP - 2) % EP, tp)

    def sibling(origin):
        block = 2 * origin + core
        return remote(kv.at[block], kv.at[block], sib_s.at[origin], sib_r.at[origin], sib, tp)

    def sibling_in(origin):
        block = 2 * origin + 1 - core
        return remote(kv.at[block], kv.at[block], sib_s.at[origin], sib_r.at[origin], sib, tp)

    far = 6

    def ring_open():
        @pl.when(z < CHIPS - 1)
        def _():
            plus(0).start()

        @pl.when(z <= far)
        def _():
            minus(0).start()

        @pl.when(core == 0)
        def _():
            sibling(z).start()

    def ring_step(d):
        @pl.when(z - d >= 0)
        def _():
            plus_in(d).wait_recv()
            if d < 8:
                @pl.when(z < CHIPS - 1)
                def _():
                    plus(d).start()
            sibling(z - d).start()

        if d <= 7:
            origin = (z + d) % CHIPS

            @pl.when(origin <= far)
            def _():
                minus_in(d).wait_recv()
                if d < 7:
                    minus(d).start()

                @pl.when(origin < z)
                def _():
                    sibling(origin).start()

    ring_open()

    xrec[ep] = xsend[ep]

    def dispatch_wait(i, carry):
        source = (ep + i) % EP
        remote(xsend.at[source], xrec.at[source], d_s.at[i], d_r.at[source], source, tp).wait_recv()
        return carry

    lax.fori_loop(1, EP, dispatch_wait, 0)
    pack = pack_ref[...]
    for h in range(2):
        got = jnp.concatenate([xrec[h * (EP // 2) + s] for s in range(EP // 2)], axis=0)
        xall[h * HALF : (h + 1) * HALF, lanes(tp)] = mm(pack, got).astype(BF16)

    top, low = pl.ds(0, HALF), pl.ds(HALF, HALF)

    def ag1(h, j):
        part = xall.at[(top, low)[h], lanes(tp)]
        return remote(part, part, ag1_s.at[h, j], ag1_r.at[h, j], ep, x_peer(j) if h == 0 else y_peer(j))

    def ag1_in(h, j):
        other = x_peer(SIDE - j) if h == 0 else y_peer(SIDE - j)
        part = xall.at[(top, low)[h], lanes(other)]
        return remote(part, part, ag1_s.at[h, j], ag1_r.at[h, j], ep, other)

    for j in (2, 1, 3):
        for h in range(2):
            ag1(h, j).start()
    ring_step(1)

    def ag2a(j, row):
        part = xall.at[top, lanes(row, BAND)]
        return remote(part, part, ag2_s.at[0, j], ag2_r.at[0, j], ep, y_peer(j))

    def ag2b(j, n, column):
        part = xall.at[low, lanes(n * SIDE + column)]
        return remote(part, part, ag2_s.at[1 + n, j], ag2_r.at[1 + n, j], ep, x_peer(j))

    for j in (1, 3, 2):
        ag1_in(0, j).wait_recv()
    for j in (2, 1, 3):
        ag2a(j, y).start()
    for j in (1, 3, 2):
        ag1_in(1, j).wait_recv()
    for j in (2, 1, 3):
        for n in range(SIDE):
            ag2b(j, n, x).start()
    ring_step(2)
    ring_step(3)
    ring_step(4)
    ring_step(5)

    for copy in weight_copies:
        copy.wait()

    def ffn(i, carry):
        rows = pl.ds(pl.multiple_of(i * TILE, TILE), TILE)
        block = xall[rows, :]
        gated = jnp.minimum(mm(block, gate_ref[...]), CLAMP_LIMIT)
        clipped = jnp.clip(mm(block, up_ref[...]), -CLAMP_LIMIT, CLAMP_LIMIT)
        active = ((clipped + 1.0) * gated * jax.nn.sigmoid(GATE_SLOPE * gated)).astype(BF16)
        ypart[rows, :] = mm(active, down_ref[...]).astype(BF16)
        return carry

    def rs1_a(j):
        to = (y + j) % SIDE
        return remote(ypart.at[top, lanes(to, BAND)], rs1a.at[j - 1], r1_s.at[0, j], r1_r.at[0, j], ep, y_peer(j))

    def rs1_b(j, n):
        to = (x + j) % SIDE
        return remote(
            ypart.at[low, lanes(n * SIDE + to)], rs1b.at[j - 1, n], r1_s.at[1 + n, j], r1_r.at[1 + n, j], ep, x_peer(j)
        )

    for j in (1, 3, 2):
        ag2a(j, (y + SIDE - j) % SIDE).wait_recv()
    lax.fori_loop(0, HALF // TILE, ffn, 0)
    for j in (2, 1, 3):
        rs1_a(j).start()
    for j in (1, 3, 2):
        for n in range(SIDE):
            ag2b(j, n, (x + SIDE - j) % SIDE).wait_recv()
    lax.fori_loop(HALF // TILE, 2 * HALF // TILE, ffn, 0)
    for j in (2, 1, 3):
        for n in range(SIDE):
            rs1_b(j, n).start()

    ring_step(6)
    ring_step(7)
    ring_step(8)

    column = lax.broadcasted_iota(jnp.int32, (TOK, LANE), 1)
    row = lax.broadcasted_iota(jnp.int32, (TOK, LANE), 0)
    query = qkv_ref[0] * jnp.asarray(0.125, BF16)
    nothing = jnp.zeros_like(query)
    queries = jnp.concatenate([jnp.where(column < 64, query, nothing), jnp.where(column < 64, nothing, query)], axis=0)
    causal = jnp.concatenate([column <= row, column <= row], axis=0)

    scores = jnp.where(causal, mm(queries, kv[ep, 0], NT), -jnp.inf)
    top_score = jnp.max(scores, axis=-1, keepdims=True)
    terms = jnp.exp(scores - top_score)
    m_ref[...] = jnp.broadcast_to(top_score, (2 * TOK, LANE))
    l_ref[...] = jnp.broadcast_to(jnp.sum(terms, axis=-1, keepdims=True), (2 * TOK, LANE))
    acc_ref[...] = mm(terms.astype(BF16), kv[ep, 1])

    def attend(keys, values):
        scores = mm(queries, keys, NT)
        old = m_ref[:, 0:1]
        new = jnp.maximum(old, jnp.max(scores, axis=-1, keepdims=True))
        shrink = jnp.exp(old - new)
        terms = jnp.exp(scores - new)
        m_ref[...] = jnp.broadcast_to(new, (2 * TOK, LANE))
        l_ref[...] = l_ref[...] * shrink + jnp.sum(terms, axis=-1, keepdims=True)
        acc_ref[...] = acc_ref[...] * shrink + mm(terms.astype(BF16), values)

    @pl.when(core == 1)
    def _():
        sibling_in(z).wait_recv()
        attend(kv[2 * z, 0], kv[2 * z, 1])

    def attend_chip(origin, carry):
        sibling_in(origin).wait_recv()
        keys = jnp.concatenate([kv[2 * origin, 0], kv[2 * origin + 1, 0]], axis=0)
        values = jnp.concatenate([kv[2 * origin, 1], kv[2 * origin + 1, 1]], axis=0)
        attend(keys, values)
        return carry

    lax.fori_loop(0, z, attend_chip, 0)
    ratio = acc_ref[...] / l_ref[...]
    attended = ratio[:TOK] - lam_ref[...] * ratio[TOK:]
    square = jnp.mean(attended * attended, axis=-1, keepdims=True)
    head = (attended * lax.rsqrt(square + NORM_EPS) * gain_ref[...]).astype(BF16)
    product = mm(head, ow_ref[...])
    for t in range(TP):
        psend[t] = product[t * 8 : (t + 1) * 8].astype(BF16)

    def share(i):
        peer = (tp + i) % TP
        return remote(psend.at[peer], prec.at[tp], p_s.at[i], p_r.at[tp], ep, peer)

    def share_start(i, carry):
        share(i).start()
        return carry

    lax.fori_loop(1, TP, share_start, 0)
    prec[tp] = psend[tp]

    def rs2_a(j):
        to = (x + j) % SIDE
        return remote(z0.at[:, lanes(to)], rs2a.at[j - 1], r2_s.at[0, j], r2_r.at[0, j], ep, x_peer(j))

    def rs2_b(j):
        to = (y + j) % SIDE
        return remote(z1.at[to], rs2b.at[j - 1], r2_s.at[1, j], r2_r.at[1, j], ep, y_peer(j))

    for j in (1, 3, 2):
        rs1_a(j).wait_recv()
    total = ypart[top, lanes(y, BAND)].astype(F32)
    for j in (1, 2, 3):
        total = total + rs1a[j - 1].astype(F32)
    z0[...] = total.astype(BF16)
    for j in (2, 1, 3):
        rs2_a(j).start()
    for j in (1, 3, 2):
        for n in range(SIDE):
            rs1_b(j, n).wait_recv()
    for n in range(SIDE):
        total = ypart[low, lanes(n * SIDE + x)].astype(F32)
        for j in (1, 2, 3):
            total = total + rs1b[j - 1, n].astype(F32)
        z1[n] = total.astype(BF16)
    for j in (2, 1, 3):
        rs2_b(j).start()

    unpack = unpack_ref[...]
    for j in (1, 3, 2):
        rs2_a(j).wait_recv()
    total = z0[:, lanes(x)].astype(F32)
    for j in (1, 2, 3):
        total = total + rs2a[j - 1].astype(F32)
    result = mm(unpack, total.astype(BF16)).astype(BF16)
    for s in range(EP // 2):
        rsend[s] = result[s * SLAB : (s + 1) * SLAB]
    for j in (1, 3, 2):
        rs2_b(j).wait_recv()
    total = z1[y].astype(F32)
    for j in (1, 2, 3):
        total = total + rs2b[j - 1].astype(F32)
    result = mm(unpack, total.astype(BF16)).astype(BF16)
    for s in range(EP // 2):
        rsend[EP // 2 + s] = result[s * SLAB : (s + 1) * SLAB]

    def give_back(i):
        peer = (ep + i) % EP
        return remote(rsend.at[peer], rrec.at[ep], b_s.at[i], b_r.at[ep], peer, tp)

    def give_back_start(n, carry):
        give_back(dispatch_order(n)).start()
        return carry

    lax.fori_loop(0, EP - 1, give_back_start, 0)
    rrec[ep] = rsend[ep]

    def share_wait(i, carry):
        source = (tp + i) % TP
        remote(psend.at[source], prec.at[source], p_s.at[i], p_r.at[source], ep, source).wait_recv()
        return carry

    lax.fori_loop(1, TP, share_wait, 0)
    total = prec[0].astype(F32)
    for t in range(1, TP):
        total = total + prec[t].astype(F32)
    rows_ref[...] = total.astype(BF16)

    slots = jnp.abs(mm(place.astype(BF16), spread, NT)) < 0.5
    parts = []
    rest = weight
    for _ in range(3):
        part = rest.astype(BF16)
        rest = rest - part.astype(F32)
        parts.append(jnp.where(slots, mm(part, spread, NT), 0.0).astype(BF16))

    def give_back_wait(i, carry):
        source = (ep + i) % EP
        remote(rsend.at[source], rrec.at[source], b_s.at[i], b_r.at[source], source, tp).wait_recv()
        return carry

    lax.fori_loop(1, EP, give_back_wait, 0)
    back = jnp.concatenate([rrec[e] for e in range(EP)], axis=0)
    combined = mm(parts[2], back) + mm(parts[1], back) + mm(parts[0], back)
    experts_ref[...] = combined.astype(BF16)

    def drain_ep(i, carry):
        dispatch(i).wait_send()
        give_back(i).wait_send()
        return carry

    lax.fori_loop(1, EP, drain_ep, 0)

    def drain_tp(i, carry):
        share(i).wait_send()
        return carry

    lax.fori_loop(1, TP, drain_tp, 0)
    for j in (1, 2, 3):
        for h in range(2):
            ag1(h, j).wait_send()
        ag2a(j, y).wait_send()
        rs1_a(j).wait_send()
        rs2_a(j).wait_send()
        rs2_b(j).wait_send()
        for n in range(SIDE):
            ag2b(j, n, x).wait_send()
            rs1_b(j, n).wait_send()
    for d in range(8):
        @pl.when((z < CHIPS - 1) & (z - d >= 0))
        def _():
            plus(d).wait_send()
    for d in range(7):
        @pl.when((z + d) % CHIPS <= far)
        def _():
            minus(d).wait_send()

    def drain_sibling(origin, carry):
        sibling(origin).wait_send()
        return carry

    lax.fori_loop(0, z + (1 - core), drain_sibling, 0)


def body(
    query_maps, key_maps, value_rows, head_lambda, head_gain, out_weight, token_rows, norm_gain, expert_ids,
    route_weights, gate_weight, up_weight, down_weight,
):
    qkv = jnp.stack([a.reshape(TOK, LANE) for a in (query_maps, key_maps, value_rows)])
    spread, pack, unpack = (jnp.asarray(a, BF16) for a in slot_tables())
    vmem = pl.BlockSpec(memory_space=pltpu.VMEM)
    hbm = pl.BlockSpec(memory_space=pl.ANY)
    dma = pltpu.SemaphoreType.DMA
    return pl.pallas_call(
        kernel,
        name="layer",
        out_shape=(jax.ShapeDtypeStruct((TOK // TP, D), BF16), jax.ShapeDtypeStruct((TOK, LANE), BF16)),
        in_specs=[vmem, vmem, vmem, hbm] + [vmem] * 7 + [hbm] * 3,
        out_specs=(vmem, vmem),
        scratch_shapes=[
            pltpu.VMEM((EP, 2, TOK, LANE), BF16),
            pltpu.VMEM((2 * TOK, LANE), F32),
            pltpu.VMEM((2 * TOK, LANE), F32),
            pltpu.VMEM((2 * TOK, LANE), F32),
            pltpu.VMEM((TP, TOK // TP, D), BF16),
            pltpu.VMEM((TP, TOK // TP, D), BF16),
            pltpu.VMEM((EP, SLAB, LANE), BF16),
            pltpu.VMEM((EP, SLAB, LANE), BF16),
            pltpu.VMEM((ROWS, D), BF16),
            pltpu.VMEM((ROWS, D), BF16),
            pltpu.VMEM((SIDE - 1, HALF, BAND), BF16),
            pltpu.VMEM((SIDE - 1, SIDE, HALF, LANE), BF16),
            pltpu.VMEM((HALF, BAND), BF16),
            pltpu.VMEM((SIDE, HALF, LANE), BF16),
            pltpu.VMEM((SIDE - 1, HALF, LANE), BF16),
            pltpu.VMEM((SIDE - 1, HALF, LANE), BF16),
            pltpu.VMEM((EP, SLAB, LANE), BF16),
            pltpu.VMEM((EP, SLAB, LANE), BF16),
            pltpu.VMEM((LANE, D), BF16),
            pltpu.VMEM((D, UNITS), BF16),
            pltpu.VMEM((D, UNITS), BF16),
            pltpu.VMEM((UNITS, D), BF16),
            dma((4,)),
            dma((8,)), dma((9,)), dma((7,)), dma((8,)), dma((CHIPS,)), dma((CHIPS,)),
            dma((TP,)), dma((TP,)), dma((EP,)), dma((EP,)),
            dma((2, SIDE)), dma((2, SIDE)), dma((1 + SIDE, SIDE)), dma((1 + SIDE, SIDE)),
            dma((1 + SIDE, SIDE)), dma((1 + SIDE, SIDE)), dma((2, SIDE)), dma((2, SIDE)),
            dma((EP,)), dma((EP,)),
        ],
        compiler_params=pltpu.CompilerParams(
            collective_id=0, has_side_effects=True, vmem_limit_bytes=60 * 1024 * 1024
        ),
    )(
        qkv, head_lambda.reshape(1, 1), head_gain.reshape(1, LANE), out_weight, token_rows,
        norm_gain.reshape(1, D), expert_ids, route_weights, spread, pack, unpack,
        gate_weight.reshape(D, UNITS), up_weight.reshape(D, UNITS), down_weight.reshape(UNITS, D),
    )


def solution(mesh):
    placed = (
        P("ep", "tp", None), P("ep", "tp", None), P("ep", "tp", None), P("tp"), P(), P("tp", None), P("ep", None),
        P(), P("ep", None), P("ep", None), P("ep", None, "tp"), P("ep", None, "tp"), P("ep", "tp", None),
    )
    return jax.shard_map(
        body, mesh=mesh, in_specs=placed, out_specs=(P(("ep", "tp"), None), P("ep", "tp")), check_vma=False
    )
```

time: 210 us -> 103 us (0.49)
  Pallas kernels: 0 us -> 96.9 us
  waiting for transfers between devices: 53.7 us -> 0 us
  blocking collectives: 39.4 us -> 0 us
  starting transfers between devices: 38.2 us -> 0 us
  local copies, waits for them, and re-layouts: 30.8 us -> 4.2 us
  matrix products: 15.2 us -> 0 us
  between operations: 16.3 us -> 1.31 us
  other arithmetic: 14.7 us -> 0.65 us
    pallas_call x0 -> x1, Pallas kernels: none -> 96.9 us  [body(): pl.pallas_call(kernel, name='layer', out_shape=(jax.ShapeDtypeStruct((TOK...]
    all_to_all x4 -> x0, waiting for transfers between devices: 53.7 us -> none  [the longest x1 18 us: expert_half(): lax.all_to_all(outgoing_part, 'ep', split_axis=0, concat_axis=0, tiled=True)]
    all_to_all x1 -> x0, blocking collectives: 39.4 us -> none  [sent_to_all(): lax.all_to_all(jnp.broadcast_to(array[None], (length, *array.shape)), axi...]
    all_to_all x4 -> x0, starting transfers between devices: 38.2 us -> none  [the longest x1 16.7 us: expert_half(): lax.all_to_all(outgoing_part, 'ep', split_axis=0, concat_axis=0, tiled=True)]
    dot_general x11 -> x0, matrix products: 15.2 us -> none  [the longest x1 6.09 us: complete_experts(): jnp.einsum('scf,fd->scd', active, down_matrix, preferred_element_type=jnp...]
    reduce_sum x10 -> x0, other arithmetic: 8.38 us -> none  [the longest x2 2.81 us: sum_at_owner(): return arrived.astype(jnp.float32).sum(axis=0)]
    gather x2 -> x0, local copies, waits for them, and re-layouts: 5.43 us -> none  [the longest x1 4.09 us: expert_half(): outgoing = padded[slot_table].reshape(expert_count, capacity, model_width)]
    reshape x2 -> x0, local copies, waits for them, and re-layouts: 5.24 us -> none  [the longest x1 5.21 us: expert_half(): outgoing = padded[slot_table].reshape(expert_count, capacity, model_width)]
  transfers between devices with their start and end apart: 5 -> 0, of which waited for: 4 -> 0; matrix products, arithmetic and copies ran while one was open for 18% -> 0% of each run, Pallas kernels for 0% -> 0%
where the time goes in v1:
time: 103 us
  Pallas kernels  96.9 us (94%)
  local copies, waits for them, and re-layouts  4.2 us (4%)
  between operations  1.31 us (1%)
    pallas_call x1, Pallas kernels, body(): pl.pallas_call(kernel, name='layer', out_shape=(jax.ShapeDtypeStruct((TOK...  96.9 us
    unnamed x16, local copies, waits for them, and re-layouts  4.2 us

profile of v1, /device:TPU:1, one launch (start us, length us, event | category | flops | bytes accessed | tf_op | source)
XLA Modules:
  0.0 103.0 jit_solution(2988939251166672673)
XLA Ops:
  1.3 0.0 copy-start.4
  1.3 0.7 copy-done.4
  2.0 0.0 copy-start.5
  2.0 0.0 copy-start.3
  2.0 0.7 copy.18.ids_ref
  2.7 0.0 copy-done.5
  2.7 0.0 copy-start.1
  2.7 0.0 copy-start.2
  2.7 0.7 copy.19.wts_ref
  3.4 0.0 copy-done.3
  3.4 0.0 copy-done.1
  3.5 0.0 copy-done.2
  3.5 0.7 pad_maximum_fusion.qkv_ref
  4.1 96.9 %layer.1 = (bf16[8,2048]{1,0:T(8,128)(2,1)}, bf16[128,128]{1,0:T(8,128)(2,1)}) custom-call(bf16[3,128,128]{2,1,0:T(8,128)(2,1)} %pad_maximum_fusion.qkv_ref, f32[1,1]{1,0:T(1,128)} %bitcast.9.lam_ref, f32[1,128]{1,0:T(1,128)} %bitcast.17, bf16[128,2048]{1,0:T(8,128)(2,1)} %ow_hbm.1, bf16[128,2048]{1,0:T(8,128)(2,1)} %tok_ref.1, f32[1,2048]{1,0:T(1,128)} %bitcast.16, ...), custom_call_target="tpu_custom_call" | custom-call | tf_op jit(solution)/shard_map/layer/pallas_call | solution.py:474
  101.0 0.0 copy-start
  101.0 1.4 %copy.23 = bf16[8,2048]{1,0:T(8,128)(2,1)} copy(bf16[8,2048]{1,0:T(8,128)(2,1)} %get-tuple-element.4) | data formatting | bytes 65536
  102.4 0.0 copy-done
  102.4 0.6 copy.24
Async XLA Ops:
  1.3 0.7 copy-start.4
  2.0 0.7 copy-start.5
  2.0 1.5 %copy-start.3 = (bf16[128,1,128]{2,0,1:T(8,128)(2,1)S(1)}, bf16[128,1,128]{2,0,1:T(8,128)(2,1)}, u32[]{:S(2)}) copy-start(bf16[128,1,128]{2,0,1:T(8,128)(2,1)} %param.16) | copy-start | bytes 98308
  2.7 0.8 copy-start.1
  2.7 0.8 copy-start.2
  101.0 1.4 %copy-start = (bf16[128,128]{1,0:T(8,128)(2,1)S(1)}, bf16[128,128]{1,0:T(8,128)(2,1)}, u32[]{:S(2)}) copy-start(bf16[128,128]{1,0:T(8,128)(2,1)} %get-tuple-element.5) | copy-start | bytes 98308

commit v2 on v1

v2 whole, which is shorter than its diff:
```python
import functools

import jax
import jax.numpy as jnp
import numpy as np
from jax import lax
from jax.experimental import pallas as pl
from jax.experimental.pallas import tpu as pltpu
from jax.sharding import PartitionSpec as P

NORM_EPS = 1e-05
CLAMP_LIMIT = 7.0
GATE_SLOPE = 1.702
MESH = pl.DeviceIdType.MESH

EP, TP, SIDE, CHIPS = 32, 16, 4, 16
CAP, SLAB = 20, 24
CHUNKS = ((0, 1, 15, 2), (12, 5, 11, 6), (10, 7, 9, 8), (14, 3, 13, 4))
STEPS = len(CHUNKS)
SOURCES = EP // STEPS
ROWS = EP * CAP
TILE, PADDED_TILE = SOURCES * CAP, SOURCES * SLAB
HALF = TILE // 2
PADDED = EP * SLAB
D, LANE, TOK, UNITS = 2048, 128, 128, 256
BAND = SIDE * LANE
PAIR = 2 * LANE
FAR = 6
F32, BF16 = jnp.float32, jnp.bfloat16
NN = (((1,), (0,)), ((), ()))
NT = (((1,), (1,)), ((), ()))


def mm(a, b, dims=NN):
    return lax.dot_general(a, b, dims, preferred_element_type=F32)


def slot_tables():
    rows = np.arange(PADDED)
    spread = np.zeros((PADDED, LANE), np.float32)
    spread[rows, rows // SLAB] = 1.0
    spread[rows, EP] = -(rows % SLAB)
    pack = np.zeros((TILE, PADDED_TILE), np.float32)
    r = np.arange(TILE)
    pack[r, r // CAP * SLAB + r % CAP] = 1.0
    return spread, pack, pack.T.copy()


def kernel(
    q_hbm, k_hbm, v_hbm, lam_hbm, gain_hbm, ow_hbm, tok_hbm, ngain_hbm, ids_hbm, wts_hbm, spread_hbm, pack_hbm,
    unpack_hbm, gate_hbm, up_hbm, down_hbm,
    rows_ref, experts_ref,
    q_ref, lam_ref, gain_ref, ow_ref, tok_ref, ngain_ref, ids_ref, wts_ref, spread_ref, pack_ref, unpack_ref,
    gate_ref, up_ref, down_ref,
    kv, m_ref, l_ref, acc_ref, ps, pa, pb, pc, xsend, xrec, xall, ypart, rs1, comb, band, rs2, rsend, rrec,
    local_sem, plus_s, plus_r, minus_s, minus_r, sib_s, sib_r, sent, p_r, d_r, ag1_r, ag2_r, ag2_rest, r1_r, r1_rest,
    r2_r, b_r,
):
    ep = lax.axis_index("ep")
    tp = lax.axis_index("tp")
    z, core = ep // 2, ep % 2
    x, y = tp % SIDE, tp // SIDE
    sib = z * 2 + (1 - core)

    def lanes(block, width=LANE):
        return pl.ds(pl.multiple_of(block * width, width), width)

    def remote(src, dst, ssem, rsem, e, t):
        return pltpu.make_async_remote_copy(
            src_ref=src, dst_ref=dst, send_sem=ssem, recv_sem=rsem, device_id=(e, t), device_id_type=MESH
        )

    def arrived(ref, sem):
        remote(ref, ref, sent.at[0], sem, sib, tp).wait_recv()

    def left(ref, kind):
        remote(ref, ref, sent.at[kind], b_r.at[0], sib, tp).wait_send()

    def x_peer(j):
        return y * SIDE + (x + j) % SIDE

    def y_peer(j):
        return ((y + j) % SIDE) * SIDE + x

    barrier = pltpu.get_barrier_semaphore()

    def greet_ep(n, carry):
        off = (n + 1) // 2
        to = (ep + EP // 2 + off * (1 - 2 * (n % 2))) % EP
        pl.semaphore_signal(barrier, inc=1, device_id=(to, tp), device_id_type=MESH)
        return carry

    def greet_tp(i, carry):
        pl.semaphore_signal(barrier, inc=1, device_id=(ep, (tp + i) % TP), device_id_type=MESH)
        return carry

    lax.fori_loop(0, EP - 1, greet_ep, 0)
    lax.fori_loop(1, TP, greet_tp, 0)

    moves = (
        (tok_hbm, tok_ref), (ids_hbm, ids_ref), (wts_hbm, wts_ref), (ngain_hbm, ngain_ref), (spread_hbm, spread_ref),
        (q_hbm, q_ref), (k_hbm, kv.at[ep, 0]), (v_hbm, kv.at[ep, 1]), (pack_hbm, pack_ref), (unpack_hbm, unpack_ref),
        (lam_hbm, lam_ref), (gain_hbm, gain_ref),
        (gate_hbm, gate_ref), (up_hbm, up_ref), (down_hbm, down_ref), (ow_hbm, ow_ref),
    )
    local = [pltpu.make_async_copy(src, dst, local_sem.at[i]) for i, (src, dst) in enumerate(moves)]
    for copy in local:
        copy.start()
    for copy in local[:5]:
        copy.wait()

    tokens = tok_ref[...].astype(F32)
    scale = lax.rsqrt(jnp.mean(tokens * tokens, axis=-1, keepdims=True) + NORM_EPS)
    mine = tok_ref[:, lanes(tp)].astype(F32)
    normed = (mine * scale * ngain_ref[:, lanes(tp)]).astype(BF16)
    first = lax.broadcasted_iota(jnp.int32, (TOK, LANE), 0)
    second = lax.broadcasted_iota(jnp.int32, (TOK, LANE), 1)
    named = jnp.zeros((TOK, LANE), F32)
    weight = jnp.zeros((TOK, LANE), F32)
    for k in range(4):
        hit = ids_ref[k : k + 1, :] == first
        named = named + jnp.where(hit, 1.0, 0.0)
        weight = weight + jnp.where(hit, wts_ref[k : k + 1, :], 0.0)
    before = jnp.where(first < second, 1.0, 0.0).astype(BF16)
    rank = mm(named.astype(BF16), before)
    place = jnp.where(named > 0.5, rank, -1.0)
    place = jnp.where(first < EP, place, jnp.where(first == EP, 1.0, 0.0))
    chosen = mm(spread_ref[...], place.astype(BF16))
    chosen = jnp.where(jnp.abs(chosen) < 0.5, 1.0, 0.0).astype(BF16)
    outgoing = mm(chosen, normed).astype(BF16)
    for e in range(EP):
        xsend[e] = outgoing[e * SLAB : (e + 1) * SLAB]
    for copy in local[5:8]:
        copy.wait()

    pl.semaphore_wait(barrier, EP - 1 + TP - 1)

    members = [[(n, chip, c) for n, chip in enumerate(CHUNKS[k]) for c in range(2)] for k in range(STEPS)]

    def elsewhere(chip, c, do):
        if chip == 0:
            pl.when(core != c)(do)
        else:
            do()

    def dispatch(k, n, chip, c):
        to = 2 * ((z + chip) % CHIPS) + c
        slot = (k * len(CHUNKS[0]) + n) * 2
        return remote(xsend.at[to], xrec.at[slot + core], sent.at[0], d_r.at[k], to, tp)

    for k in range(STEPS):
        for n, chip, c in members[k]:
            elsewhere(chip, c, lambda: dispatch(k, n, chip, c).start())
    xrec[core] = xsend[ep]

    def plus(d):
        block = 2 * (z - d) + core
        return remote(kv.at[block], kv.at[block], plus_s.at[d], plus_r.at[d + 1], (ep + 2) % EP, tp)

    def plus_in(d):
        block = 2 * (z - d) + core
        return remote(kv.at[block], kv.at[block], plus_s.at[d - 1], plus_r.at[d], (ep + 2) % EP, tp)

    def minus(d):
        block = 2 * ((z + d) % CHIPS) + core
        return remote(kv.at[block], kv.at[block], minus_s.at[d], minus_r.at[d + 1], (ep + EP - 2) % EP, tp)

    def minus_in(d):
        block = 2 * ((z + d) % CHIPS) + core
        return remote(kv.at[block], kv.at[block], minus_s.at[d - 1], minus_r.at[d], (ep + EP - 2) % EP, tp)

    def sibling(origin):
        block = 2 * origin + core
        return remote(kv.at[block], kv.at[block], sib_s.at[origin], sib_r.at[origin], sib, tp)

    def sibling_in(origin):
        block = 2 * origin + 1 - core
        return remote(kv.at[block], kv.at[block], sib_s.at[origin], sib_r.at[origin], sib, tp)

    def ring_open():
        @pl.when(z < CHIPS - 1)
        def _():
            plus(0).start()

        @pl.when(z <= FAR)
        def _():
            minus(0).start()

        @pl.when(core == 0)
        def _():
            sibling(z).start()

    def ring_step(d):
        @pl.when(z - d >= 0)
        def _():
            plus_in(d).wait_recv()
            if d < 8:
                @pl.when(z < CHIPS - 1)
                def _():
                    plus(d).start()
            sibling(z - d).start()

        if d <= 7:
            origin = (z + d) % CHIPS

            @pl.when(origin <= FAR)
            def _():
                minus_in(d).wait_recv()
                if d < 7:
                    minus(d).start()

                @pl.when(origin < z)
                def _():
                    sibling(origin).start()

    far_first = (2, 1, 3)

    queries_of = []

    def attend(blocks):
        keys = jnp.concatenate([kv[b, 0] for b in blocks], axis=0)
        values = jnp.concatenate([kv[b, 1] for b in blocks], axis=0)
        scores = mm(queries_of[0], keys, NT)
        old = m_ref[:, 0:1]
        new = jnp.maximum(old, jnp.max(scores, axis=-1, keepdims=True))
        shrink = jnp.exp(old - new)
        terms = jnp.exp(scores - new)
        m_ref[...] = jnp.broadcast_to(new, (2 * TOK, LANE))
        l_ref[...] = l_ref[...] * shrink + jnp.sum(terms, axis=-1, keepdims=True)
        acc_ref[...] = acc_ref[...] * shrink + mm(terms.astype(BF16), values)

    def attend_open():
        query = q_ref[...] * jnp.asarray(0.125, BF16)
        nothing = jnp.zeros_like(query)
        queries = jnp.concatenate([jnp.where(second < 64, query, nothing), jnp.where(second < 64, nothing, query)], axis=0)
        queries_of.append(queries)
        causal = jnp.concatenate([second <= first, second <= first], axis=0)
        scores = jnp.where(causal, mm(queries, kv[ep, 0], NT), -jnp.inf)
        top_score = jnp.max(scores, axis=-1, keepdims=True)
        terms = jnp.exp(scores - top_score)
        m_ref[...] = jnp.broadcast_to(top_score, (2 * TOK, LANE))
        l_ref[...] = jnp.broadcast_to(jnp.sum(terms, axis=-1, keepdims=True), (2 * TOK, LANE))
        acc_ref[...] = mm(terms.astype(BF16), kv[ep, 1])

    def attend_pair():
        @pl.when(core == 1)
        def _():
            sibling_in(z).wait_recv()
            attend([2 * z])

    def attend_some(a, a_in, b, b_in):
        def both():
            sibling_in(a).wait_recv()
            sibling_in(b).wait_recv()
            attend([2 * a, 2 * a + 1, 2 * b, 2 * b + 1])

        def one():
            sibling_in(a).wait_recv()
            attend([2 * a, 2 * a + 1])

        pl.when(a_in & b_in)(both)
        pl.when(a_in & jnp.logical_not(b_in))(one)

    def attend_plus(d):
        attend_some(z - d, z - d >= 0, z - d - 1, z - d - 1 >= 0)

    def attend_minus(d):
        late, early = (z + d + 1) % CHIPS, (z + d) % CHIPS
        attend_some(late, z + d + 1 >= CHIPS, early, z + d >= CHIPS)

    def attend_last():
        origin = (z + 7) % CHIPS

        @pl.when(z + 7 >= CHIPS)
        def _():
            sibling_in(origin).wait_recv()
            attend([2 * origin, 2 * origin + 1])

    def attend_close():
        ratio = acc_ref[...] / l_ref[...]
        attended = ratio[:TOK] - lam_ref[...] * ratio[TOK:]
        square = jnp.mean(attended * attended, axis=-1, keepdims=True)
        head = (attended * lax.rsqrt(square + NORM_EPS) * gain_ref[...]).astype(BF16)
        product = mm(head, ow_ref[...])
        for q in range(SIDE):
            ps[0, q] = product[q * 32 : (q + 1) * 32, : D // 2].astype(BF16)
            picked = [product[(n * SIDE + q) * 8 : (n * SIDE + q) * 8 + 8, D // 2 :] for n in range(SIDE)]
            ps[1, q] = jnp.concatenate(picked, axis=0).astype(BF16)
        for j in far_first:
            for h in range(2):
                share_first(h, j).start()

    def share_first(h, j):
        to = (second_at[h] + j) % SIDE
        return remote(ps.at[h, to], pa.at[h, j - 1], sent.at[6], p_r.at[0], ep, along(h, j))

    def share_second(h, j):
        to = (first_at[h] + j) % SIDE
        return remote(pb.at[h, to], pc.at[h, j - 1], sent.at[7], p_r.at[1], ep, across(h, j))

    def share_sum():
        arrived(pa, p_r.at[0])
        for h in range(2):
            total = ps[h, second_at[h]].astype(F32)
            for j in (1, 2, 3):
                total = total + pa[h, j - 1].astype(F32)
            for n in range(SIDE):
                pb[h, n] = total[n * 8 : (n + 1) * 8].astype(BF16)
            for j in far_first:
                share_second(h, j).start()

    def rows(k, h):
        return pl.ds(k * TILE + h * HALF, HALF)

    def ag1(k, h, j):
        part = xall.at[rows(k, h), lanes(tp)]
        return remote(part, part, sent.at[1], ag1_r.at[k], ep, x_peer(j) if h == 0 else y_peer(j))

    second_at = (y, x)
    first_at = (x, y)

    def along(h, j):
        return y_peer(j) if h == 0 else x_peer(j)

    def across(h, j):
        return x_peer(j) if h == 0 else y_peer(j)

    def columns(h, q, half):
        q = q % SIDE
        if h == 0:
            return [lanes(2 * q + half, PAIR)]
        return [lanes((2 * half + i) * SIDE + q) for i in range(2)]

    def pieces(h):
        return range(1 + h)

    def ahead(s):
        return 1 if s == 0 else SIDE - 1

    def behind(s):
        return SIDE - ahead(s)

    def ag2(k, h, s, half, i, q):
        part = xall.at[rows(k, h), columns(h, q, half)[i]]
        sem = ag2_r.at[k, h, s] if half == s else ag2_rest.at[k]
        return remote(part, part, sent.at[2], sem, ep, along(h, ahead(s)))

    def ag2_relay(k, h, s, i, q):
        part = xall.at[rows(k, h), columns(h, q, s)[i]]
        return remote(part, part, sent.at[2], ag2_rest.at[k], ep, along(h, ahead(s)))

    def rs1_raw(k, h, s, kind, i):
        q, half = (second_at[h] + 2, s) if kind == 0 else (second_at[h] + ahead(s), 1 - s)
        part = ypart.at[rows(k, h), columns(h, q, half)[i]]
        to = rs1.at[k, h, kind, s] if h == 0 else rs1.at[k, h, kind, s, :, pl.ds(i * LANE, LANE)]
        sem = r1_r.at[k, h, s] if kind == 0 else r1_rest.at[k, h]
        return remote(part, to, sent.at[3], sem, ep, along(h, ahead(s)))

    def rs1_comb(k, h, s):
        return remote(comb.at[k, h, s], rs1.at[k, h, 2, s], sent.at[3], r1_rest.at[k, h], ep, along(h, ahead(s)))

    def share_of(k, h, q, half):
        return jnp.concatenate([ypart[rows(k, h), c].astype(F32) for c in columns(h, q, half)], axis=1)

    def rs2_copy(k, h, j):
        part = band.at[k, h, :, lanes((first_at[h] + j) % SIDE)]
        return remote(part, rs2.at[k, h, j - 1], sent.at[4], r2_r.at[k], ep, across(h, j))

    def give_back(k, n, chip, c):
        to = 2 * ((z + CHIPS - chip) % CHIPS) + c
        slot = (k * len(CHUNKS[0]) + n) * 2 + c
        return remote(rsend.at[slot], rrec.at[ep], sent.at[5], b_r.at[0], to, tp)


    def gather_open(k):
        arrived(xrec.at[pl.ds(k * SOURCES, SOURCES - (k == 0))], d_r.at[k])
        got = jnp.concatenate([xrec[k * SOURCES + s] for s in range(SOURCES)], axis=0)
        xall[k * TILE : (k + 1) * TILE, lanes(tp)] = mm(pack_ref[...], got).astype(BF16)
        for j in far_first:
            for h in range(2):
                ag1(k, h, j).start()

    def gather_more(k):
        arrived(xall.at[pl.ds(k * TILE, TILE), pl.ds(0, (SIDE - 1) * LANE)], ag1_r.at[k])
        for turn in range(2):
            for h in range(2):
                for s in range(2):
                    for i in pieces(h):
                        ag2(k, h, s, (s + turn) % 2, i, second_at[h]).start()

    def gather_relay(k):
        for h in range(2):
            for s in range(2):
                arrived(xall.at[rows(k, h), pl.ds(0, PAIR)], ag2_r.at[k, h, s])
                for i in pieces(h):
                    ag2_relay(k, h, s, i, second_at[h] + behind(s)).start()

    def experts(k):
        arrived(xall.at[pl.ds(k * TILE, TILE), pl.ds(0, 4 * PAIR)], ag2_rest.at[k])
        block = xall[k * TILE : (k + 1) * TILE, :]
        gated = jnp.minimum(mm(block, gate_ref[...]), CLAMP_LIMIT)
        clipped = jnp.clip(mm(block, up_ref[...]), -CLAMP_LIMIT, CLAMP_LIMIT)
        active = ((clipped + 1.0) * gated * jax.nn.sigmoid(GATE_SLOPE * gated)).astype(BF16)
        ypart[k * TILE : (k + 1) * TILE, :] = mm(active, down_ref[...]).astype(BF16)
        for kind in range(2):
            for h in range(2):
                for s in range(2):
                    for i in pieces(h):
                        rs1_raw(k, h, s, kind, i).start()

    def sum_relay(k):
        for h in range(2):
            for s in range(2):
                arrived(rs1.at[k, h, 0, s], r1_r.at[k, h, s])
                own = share_of(k, h, second_at[h] + ahead(s), s)
                comb[k, h, s] = (own + rs1[k, h, 0, s].astype(F32)).astype(BF16)
                rs1_comb(k, h, s).start()

    def sum_open(k):
        for h in range(2):
            arrived(rs1.at[k, h, pl.ds(1, 2)], r1_rest.at[k, h])
            for half in range(2):
                own = share_of(k, h, second_at[h], half)
                total = own + rs1[k, h, 2, half].astype(F32) + rs1[k, h, 1, 1 - half].astype(F32)
                band[k, h, :, half * PAIR : (half + 1) * PAIR] = total.astype(BF16)
            for j in far_first:
                rs2_copy(k, h, j).start()

    def sum_close(k):
        halves = []
        arrived(rs2.at[k], r2_r.at[k])
        for h in range(2):
            total = band[k, h, :, lanes(first_at[h])].astype(F32)
            for j in (1, 2, 3):
                total = total + rs2[k, h, j - 1].astype(F32)
            halves.append(total)
        total = jnp.concatenate(halves, axis=0).astype(BF16)
        result = mm(unpack_ref[...], total).astype(BF16)
        for s in range(SOURCES):
            rsend[k * SOURCES + s] = result[s * SLAB : (s + 1) * SLAB]
        for n, chip, c in members[k]:
            elsewhere(chip, c, lambda: give_back(k, n, chip, c).start())
        if k == 0:
            rrec[ep] = rsend[core]

    for copy in local[8:]:
        copy.wait()
    attend_open()
    gather_open(0)
    ring_open()
    gather_more(0)
    gather_open(1)
    ring_step(1)
    gather_relay(0)
    gather_open(2)
    gather_open(3)
    gather_more(1)
    ring_step(2)
    gather_more(2)
    experts(0)
    gather_more(3)
    attend_pair()
    ring_step(3)
    gather_relay(1)
    gather_relay(2)
    sum_relay(0)
    ring_step(4)
    attend_plus(1)
    attend_minus(1)
    experts(1)
    gather_relay(3)
    ring_step(5)
    sum_open(0)
    sum_relay(1)
    experts(2)
    ring_step(6)
    attend_plus(3)
    attend_minus(3)
    sum_close(0)
    sum_open(1)
    sum_relay(2)
    experts(3)
    ring_step(7)
    sum_close(1)
    sum_open(2)
    attend_plus(5)
    attend_minus(5)
    sum_relay(3)
    ring_step(8)
    sum_close(2)
    sum_open(3)
    attend_plus(7)
    attend_last()
    attend_close()

    places = jnp.transpose(place).astype(BF16)
    slots = jnp.abs(mm(places, spread_ref[...], NT)) < 0.5
    parts = []
    rest = jnp.transpose(weight)
    for _ in range(3):
        part = rest.astype(BF16)
        rest = rest - part.astype(F32)
        parts.append(jnp.where(slots, mm(part, spread_ref[...], NT), 0.0).astype(BF16))

    sum_close(3)
    share_sum()

    left(xsend.at[pl.ds(0, EP - 1)], 0)
    left(xall.at[pl.ds(0, TILE), pl.ds(0, 12 * LANE)], 1)
    left(xall.at[:, pl.ds(0, 12 * LANE)], 2)
    left(ypart.at[:, pl.ds(0, 12 * LANE)], 3)
    left(ypart.at[pl.ds(0, TILE), pl.ds(0, 12 * LANE)], 4)
    left(pa, 6)
    left(pc, 7)

    for d in range(8):
        @pl.when((z < CHIPS - 1) & (z - d >= 0))
        def _():
            plus(d).wait_send()
    for d in range(7):
        @pl.when((z + d) % CHIPS <= FAR)
        def _():
            minus(d).wait_send()

    def drain_sibling(origin, carry):
        sibling(origin).wait_send()
        return carry

    lax.fori_loop(0, z + (1 - core), drain_sibling, 0)

    arrived(pc, p_r.at[1])
    for h in range(2):
        total = pb[h, first_at[h]].astype(F32)
        for j in (1, 2, 3):
            total = total + pc[h, j - 1].astype(F32)
        rows_ref[:, h * (D // 2) : (h + 1) * (D // 2)] = total.astype(BF16)

    arrived(rrec.at[pl.ds(0, EP - 1)], b_r.at[0])
    back = jnp.concatenate([rrec[e] for e in range(EP)], axis=0)
    combined = mm(parts[2], back) + mm(parts[1], back) + mm(parts[0], back)
    experts_ref[...] = combined.astype(BF16)
    left(rsend.at[pl.ds(0, EP - 1)], 5)


def body(
    query_maps, key_maps, value_rows, head_lambda, head_gain, out_weight, token_rows, norm_gain, expert_ids,
    route_weights, gate_weight, up_weight, down_weight,
):
    spread, pack, unpack = (jnp.asarray(a, BF16) for a in slot_tables())
    vmem = pl.BlockSpec(memory_space=pltpu.VMEM)
    hbm = pl.BlockSpec(memory_space=pl.ANY)
    dma = pltpu.SemaphoreType.DMA
    return pl.pallas_call(
        kernel,
        name="layer",
        out_shape=(jax.ShapeDtypeStruct((TOK // TP, D), BF16), jax.ShapeDtypeStruct((TOK, LANE), BF16)),
        in_specs=[hbm] * 16,
        out_specs=(vmem, vmem),
        scratch_shapes=[
            pltpu.VMEM((TOK, LANE), BF16),
            pltpu.VMEM((1, 1), F32),
            pltpu.VMEM((1, LANE), F32),
            pltpu.VMEM((LANE, D), BF16),
            pltpu.VMEM((TOK, D), BF16),
            pltpu.VMEM((1, D), F32),
            pltpu.VMEM((4, TOK), jnp.int32),
            pltpu.VMEM((4, TOK), F32),
            pltpu.VMEM((PADDED, LANE), BF16),
            pltpu.VMEM((TILE, PADDED_TILE), BF16),
            pltpu.VMEM((PADDED_TILE, TILE), BF16),
            pltpu.VMEM((D, UNITS), BF16),
            pltpu.VMEM((D, UNITS), BF16),
            pltpu.VMEM((UNITS, D), BF16),
            pltpu.VMEM((EP, 2, TOK, LANE), BF16),
            pltpu.VMEM((2 * TOK, LANE), F32),
            pltpu.VMEM((2 * TOK, LANE), F32),
            pltpu.VMEM((2 * TOK, LANE), F32),
            pltpu.VMEM((2, SIDE, 32, D // 2), BF16),
            pltpu.VMEM((2, SIDE - 1, 32, D // 2), BF16),
            pltpu.VMEM((2, SIDE, 8, D // 2), BF16),
            pltpu.VMEM((2, SIDE - 1, 8, D // 2), BF16),
            pltpu.VMEM((EP, SLAB, LANE), BF16),
            pltpu.VMEM((EP, SLAB, LANE), BF16),
            pltpu.VMEM((ROWS, D), BF16),
            pltpu.VMEM((ROWS, D), BF16),
            pltpu.VMEM((STEPS, 2, 3, 2, HALF, PAIR), BF16),
            pltpu.VMEM((STEPS, 2, 2, HALF, PAIR), BF16),
            pltpu.VMEM((STEPS, 2, HALF, BAND), BF16),
            pltpu.VMEM((STEPS, 2, SIDE - 1, HALF, LANE), BF16),
            pltpu.VMEM((EP, SLAB, LANE), BF16),
            pltpu.VMEM((EP, SLAB, LANE), BF16),
            dma((16,)),
            dma((8,)), dma((9,)), dma((7,)), dma((8,)), dma((CHIPS,)), dma((CHIPS,)),
            dma((8,)), dma((2,)), dma((STEPS,)), dma((STEPS,)), dma((STEPS, 2, 2)), dma((STEPS,)), dma((STEPS, 2, 2)),
            dma((STEPS, 2)), dma((STEPS,)), dma((1,)),
        ],
        compiler_params=pltpu.CompilerParams(
            collective_id=0, has_side_effects=True, vmem_limit_bytes=60 * 1024 * 1024
        ),
    )(
        query_maps.reshape(TOK, LANE), key_maps.reshape(TOK, LANE), value_rows.reshape(TOK, LANE),
        head_lambda.reshape(1, 1), head_gain.reshape(1, LANE), out_weight, token_rows, norm_gain.reshape(1, D),
        expert_ids.T, route_weights.T, spread, pack, unpack,
        gate_weight.reshape(D, UNITS), up_weight.reshape(D, UNITS), down_weight.reshape(UNITS, D),
    )


def solution(mesh):
    placed = (
        P("ep", "tp", None), P("ep", "tp", None), P("ep", "tp", None), P("tp"), P(), P("tp", None), P("ep", None),
        P(), P("ep", None), P("ep", None), P("ep", None, "tp"), P("ep", None, "tp"), P("ep", "tp", None),
    )
    return jax.shard_map(
        body, mesh=mesh, in_specs=placed, out_specs=(P(("ep", "tp"), None), P("ep", "tp")), check_vma=False
    )
```

time: 103 us -> 77.5 us (0.75)
  Pallas kernels: 96.9 us -> 74 us
  local copies, waits for them, and re-layouts: 4.2 us -> 2 us
    pallas_call x1, Pallas kernels: 96.9 us -> 74 us  [body(): pl.pallas_call(kernel, name='layer', out_shape=(jax.ShapeDtypeStruct((TOK...]
    unnamed x16 -> x4, local copies, waits for them, and re-layouts: 4.2 us -> 2 us
where the time goes in v2:
time: 77.5 us; the launch traced here: 77.3 us
  Pallas kernels  74 us (95%)
  local copies, waits for them, and re-layouts  2 us (3%)
  between operations  1.3 us (2%)
    pallas_call x1, Pallas kernels, body(): pl.pallas_call(kernel, name='layer', out_shape=(jax.ShapeDtypeStruct((TOK...  74 us
    unnamed x4, local copies, waits for them, and re-layouts  2 us

profile of v2, /device:TPU:1, one launch (start us, length us, event | category | flops | bytes accessed | tf_op | source)
XLA Modules:
  0.0 77.3 jit_solution(12828035799151743261)
XLA Ops:
  1.3 74.0 %layer.1 = (bf16[8,2048]{1,0:T(8,128)(2,1)}, bf16[128,128]{1,0:T(8,128)(2,1)}) custom-call(bf16[128,128]{1,0:T(8,128)(2,1)} %bitcast.15, bf16[128,128]{1,0:T(8,128)(2,1)} %bitcast.16, bf16[128,128]{1,0:T(8,128)(2,1)} %bitcast.17, f32[1,1]{1,0:T(1,128)} %bitcast.11.lam_hbm, f32[1,128]{1,0:T(1,128)} %bitcast.21, bf16[128,2048]{1,0:T(8,128)(2,1)} %ow_hbm.1, ...), custom_call_target="tpu_custom_call" | custom-call | tf_op jit(solution)/shard_map/layer/pallas_call | solution.py:553
  75.3 0.0 copy-start
  75.3 1.4 %copy.21 = bf16[8,2048]{1,0:T(8,128)(2,1)} copy(bf16[8,2048]{1,0:T(8,128)(2,1)} %get-tuple-element.4) | data formatting | bytes 65536
  76.6 0.0 copy-done
  76.6 0.6 copy.22
Async XLA Ops:
  75.3 1.4 %copy-start = (bf16[128,128]{1,0:T(8,128)(2,1)S(1)}, bf16[128,128]{1,0:T(8,128)(2,1)}, u32[]{:S(2)}) copy-start(bf16[128,128]{1,0:T(8,128)(2,1)} %get-tuple-element.5) | copy-start | bytes 98308

commit v3 on v2

--- a/solution.py
+++ b/solution.py
@@ -15,8 +15,9 @@
 
 EP, TP, SIDE, CHIPS = 32, 16, 4, 16
 CAP, SLAB = 20, 24
-CHUNKS = ((0, 1, 15, 2), (12, 5, 11, 6), (10, 7, 9, 8), (14, 3, 13, 4))
-STEPS = len(CHUNKS)
+ORDER = ((0, 1, 2, 3), (1, 0, 3, 2), (2, 0, 1, 3), (3, 0, 1, 2))
+OUTWARD = ((0, 2, 1, 3), (1, 0, 2, 3), (2, 0, 1, 3), (3, 1, 0, 2))
+STEPS = len(ORDER)
 SOURCES = EP // STEPS
 ROWS = EP * CAP
 TILE, PADDED_TILE = SOURCES * CAP, SOURCES * SLAB
@@ -135,23 +136,27 @@
 
     pl.semaphore_wait(barrier, EP - 1 + TP - 1)
 
-    members = [[(n, chip, c) for n, chip in enumerate(CHUNKS[k]) for c in range(2)] for k in range(STEPS)]
-
-    def elsewhere(chip, c, do):
-        if chip == 0:
-            pl.when(core != c)(do)
-        else:
-            do()
-
-    def dispatch(k, n, chip, c):
-        to = 2 * ((z + chip) % CHIPS) + c
-        slot = (k * len(CHUNKS[0]) + n) * 2
-        return remote(xsend.at[to], xrec.at[slot + core], sent.at[0], d_r.at[k], to, tp)
-
-    for k in range(STEPS):
-        for n, chip, c in members[k]:
-            elsewhere(chip, c, lambda: dispatch(k, n, chip, c).start())
-    xrec[core] = xsend[ep]
+    quarter = z // (CHIPS // STEPS)
+
+    def pick(table, n):
+        at = [row[n] for row in table]
+        reached = [(quarter + STEPS - i) // STEPS for i in range(1, STEPS)]
+        return at[0] + sum((at[i] - at[i - 1]) * reached[i - 1] for i in range(1, STEPS))
+
+    chunk = [pick(ORDER, k) for k in range(STEPS)]
+    outward = [pick(OUTWARD, n) for n in range(STEPS)]
+
+    def others(n):
+        return range(1 if n == 0 else 0, SOURCES)
+
+    def dispatch(n, i):
+        to = outward[n] * SOURCES + (ep + i) % SOURCES
+        return remote(xsend.at[to], xrec.at[ep], sent.at[0], d_r.at[quarter], to, tp)
+
+    for n in range(STEPS):
+        for i in others(n):
+            dispatch(n, i).start()
+    xrec[ep] = xsend[ep]
 
     def plus(d):
         block = 2 * (z - d) + core
@@ -310,7 +315,10 @@
                 share_second(h, j).start()
 
     def rows(k, h):
-        return pl.ds(k * TILE + h * HALF, HALF)
+        return pl.ds(pl.multiple_of(chunk[k] * TILE + h * HALF, HALF), HALF)
+
+    def all_rows(k):
+        return pl.ds(pl.multiple_of(chunk[k] * TILE, TILE), TILE)
 
     def ag1(k, h, j):
         part = xall.at[rows(k, h), lanes(tp)]
@@ -366,22 +374,20 @@
         part = band.at[k, h, :, lanes((first_at[h] + j) % SIDE)]
         return remote(part, rs2.at[k, h, j - 1], sent.at[4], r2_r.at[k], ep, across(h, j))
 
-    def give_back(k, n, chip, c):
-        to = 2 * ((z + CHIPS - chip) % CHIPS) + c
-        slot = (k * len(CHUNKS[0]) + n) * 2 + c
-        return remote(rsend.at[slot], rrec.at[ep], sent.at[5], b_r.at[0], to, tp)
-
+    def give_back(k, i):
+        to = chunk[k] * SOURCES + (ep + i) % SOURCES
+        return remote(rsend.at[to], rrec.at[ep], sent.at[5], b_r.at[0], to, tp)
 
     def gather_open(k):
-        arrived(xrec.at[pl.ds(k * SOURCES, SOURCES - (k == 0))], d_r.at[k])
-        got = jnp.concatenate([xrec[k * SOURCES + s] for s in range(SOURCES)], axis=0)
-        xall[k * TILE : (k + 1) * TILE, lanes(tp)] = mm(pack_ref[...], got).astype(BF16)
+        arrived(xrec.at[pl.ds(chunk[k] * SOURCES, len(others(k)))], d_r.at[chunk[k]])
+        got = jnp.concatenate([xrec[chunk[k] * SOURCES + s] for s in range(SOURCES)], axis=0)
+        xall[all_rows(k), lanes(tp)] = mm(pack_ref[...], got).astype(BF16)
         for j in far_first:
             for h in range(2):
                 ag1(k, h, j).start()
 
     def gather_more(k):
-        arrived(xall.at[pl.ds(k * TILE, TILE), pl.ds(0, (SIDE - 1) * LANE)], ag1_r.at[k])
+        arrived(xall.at[all_rows(k), pl.ds(0, (SIDE - 1) * LANE)], ag1_r.at[k])
         for turn in range(2):
             for h in range(2):
                 for s in range(2):
@@ -396,12 +402,12 @@
                     ag2_relay(k, h, s, i, second_at[h] + behind(s)).start()
 
     def experts(k):
-        arrived(xall.at[pl.ds(k * TILE, TILE), pl.ds(0, 4 * PAIR)], ag2_rest.at[k])
-        block = xall[k * TILE : (k + 1) * TILE, :]
+        arrived(xall.at[all_rows(k), pl.ds(0, 4 * PAIR)], ag2_rest.at[k])
+        block = xall[all_rows(k), :]
         gated = jnp.minimum(mm(block, gate_ref[...]), CLAMP_LIMIT)
         clipped = jnp.clip(mm(block, up_ref[...]), -CLAMP_LIMIT, CLAMP_LIMIT)
         active = ((clipped + 1.0) * gated * jax.nn.sigmoid(GATE_SLOPE * gated)).astype(BF16)
-        ypart[k * TILE : (k + 1) * TILE, :] = mm(active, down_ref[...]).astype(BF16)
+        ypart[all_rows(k), :] = mm(active, down_ref[...]).astype(BF16)
         for kind in range(2):
             for h in range(2):
                 for s in range(2):
@@ -437,11 +443,11 @@
         total = jnp.concatenate(halves, axis=0).astype(BF16)
         result = mm(unpack_ref[...], total).astype(BF16)
         for s in range(SOURCES):
-            rsend[k * SOURCES + s] = result[s * SLAB : (s + 1) * SLAB]
-        for n, chip, c in members[k]:
-            elsewhere(chip, c, lambda: give_back(k, n, chip, c).start())
+            rsend[chunk[k] * SOURCES + s] = result[s * SLAB : (s + 1) * SLAB]
+        for i in others(k):
+            give_back(k, i).start()
         if k == 0:
-            rrec[ep] = rsend[core]
+            rrec[ep] = rsend[ep]
 
     for copy in local[8:]:
         copy.wait()
@@ -451,9 +457,9 @@
     gather_more(0)
     gather_open(1)
     ring_step(1)
-    gather_relay(0)
     gather_open(2)
     gather_open(3)
+    gather_relay(0)
     gather_more(1)
     ring_step(2)
     gather_more(2)
@@ -463,35 +469,35 @@
     ring_step(3)
     gather_relay(1)
     gather_relay(2)
+    ring_step(4)
+    gather_relay(3)
     sum_relay(0)
-    ring_step(4)
     attend_plus(1)
     attend_minus(1)
+    ring_step(5)
     experts(1)
-    gather_relay(3)
-    ring_step(5)
+    experts(2)
     sum_open(0)
+    ring_step(6)
     sum_relay(1)
-    experts(2)
-    ring_step(6)
     attend_plus(3)
+    experts(3)
+    ring_step(7)
     attend_minus(3)
-    sum_close(0)
     sum_open(1)
     sum_relay(2)
-    experts(3)
-    ring_step(7)
-    sum_close(1)
-    sum_open(2)
+    sum_close(0)
+    ring_step(8)
+    sum_relay(3)
     attend_plus(5)
     attend_minus(5)
-    sum_relay(3)
-    ring_step(8)
-    sum_close(2)
-    sum_open(3)
+    sum_open(2)
+    sum_close(1)
     attend_plus(7)
     attend_last()
+    sum_open(3)
     attend_close()
+    sum_close(2)
 
     places = jnp.transpose(place).astype(BF16)
     slots = jnp.abs(mm(places, spread_ref[...], NT)) < 0.5
@@ -510,8 +516,6 @@
     left(xall.at[:, pl.ds(0, 12 * LANE)], 2)
     left(ypart.at[:, pl.ds(0, 12 * LANE)], 3)
     left(ypart.at[pl.ds(0, TILE), pl.ds(0, 12 * LANE)], 4)
-    left(pa, 6)
-    left(pc, 7)
 
     for d in range(8):
         @pl.when((z < CHIPS - 1) & (z - d >= 0))
@@ -540,6 +544,8 @@
     combined = mm(parts[2], back) + mm(parts[1], back) + mm(parts[0], back)
     experts_ref[...] = combined.astype(BF16)
     left(rsend.at[pl.ds(0, EP - 1)], 5)
+    left(pa, 6)
+    left(pc, 7)
 
 
 def body(

time: 77.5 us -> 72.7 us (0.938); the launches traced: 77.3 us -> 71.6 us
  Pallas kernels: 74 us -> 68.3 us
    pallas_call x1, Pallas kernels: 74 us -> 68.3 us  [body(): pl.pallas_call(kernel, name='layer', out_shape=(jax.ShapeDtypeStruct((TOK...]
where the time goes in v3:
time: 72.7 us; the launch traced here: 71.6 us
  Pallas kernels  68.3 us (94%)
  local copies, waits for them, and re-layouts  2 us (3%)
  between operations  1.3 us (2%)
    pallas_call x1, Pallas kernels, body(): pl.pallas_call(kernel, name='layer', out_shape=(jax.ShapeDtypeStruct((TOK...  68.3 us
    unnamed x4, local copies, waits for them, and re-layouts  2 us

profile of v3, /device:TPU:1, one launch (start us, length us, event | category | flops | bytes accessed | tf_op | source)
XLA Modules:
  0.0 71.6 jit_solution(16279511139253464116)
XLA Ops:
  1.3 68.3 %layer.1 = (bf16[8,2048]{1,0:T(8,128)(2,1)}, bf16[128,128]{1,0:T(8,128)(2,1)}) custom-call(bf16[128,128]{1,0:T(8,128)(2,1)} %bitcast.15, bf16[128,128]{1,0:T(8,128)(2,1)} %bitcast.16, bf16[128,128]{1,0:T(8,128)(2,1)} %bitcast.17, f32[1,1]{1,0:T(1,128)} %bitcast.11.lam_hbm, f32[1,128]{1,0:T(1,128)} %bitcast.21, bf16[128,2048]{1,0:T(8,128)(2,1)} %ow_hbm.1, ...), custom_call_target="tpu_custom_call" | custom-call | tf_op jit(solution)/shard_map/layer/pallas_call | solution.py:559
  69.6 0.0 copy-start
  69.6 1.4 %copy.21 = bf16[8,2048]{1,0:T(8,128)(2,1)} copy(bf16[8,2048]{1,0:T(8,128)(2,1)} %get-tuple-element.4) | data formatting | bytes 65536
  71.0 0.0 copy-done
  71.0 0.6 copy.22
Async XLA Ops:
  69.6 1.4 %copy-start = (bf16[128,128]{1,0:T(8,128)(2,1)S(1)}, bf16[128,128]{1,0:T(8,128)(2,1)}, u32[]{:S(2)}) copy-start(bf16[128,128]{1,0:T(8,128)(2,1)} %get-tuple-element.5) | copy-start | bytes 98308

commit v4 on v3

--- a/solution.py
+++ b/solution.py
@@ -27,6 +27,7 @@
 BAND = SIDE * LANE
 PAIR = 2 * LANE
 FAR = 6
+EARLY = 4
 F32, BF16 = jnp.float32, jnp.bfloat16
 NN = (((1,), (0,)), ((), ()))
 NT = (((1,), (1,)), ((), ()))
@@ -48,10 +49,10 @@
 
 
 def kernel(
-    q_hbm, k_hbm, v_hbm, lam_hbm, gain_hbm, ow_hbm, tok_hbm, ngain_hbm, ids_hbm, wts_hbm, spread_hbm, pack_hbm,
+    q_hbm, k_hbm, v_hbm, lam_ref, gain_hbm, ow_hbm, tok_hbm, ngain_hbm, ids_hbm, wts_hbm, spread_hbm, pack_hbm,
     unpack_hbm, gate_hbm, up_hbm, down_hbm,
     rows_ref, experts_ref,
-    q_ref, lam_ref, gain_ref, ow_ref, tok_ref, ngain_ref, ids_ref, wts_ref, spread_ref, pack_ref, unpack_ref,
+    q_ref, gain_ref, ow_ref, tok_ref, ngain_ref, ids_ref, wts_ref, spread_ref, pack_ref, unpack_ref,
     gate_ref, up_ref, down_ref,
     kv, m_ref, l_ref, acc_ref, ps, pa, pb, pc, xsend, xrec, xall, ypart, rs1, comb, band, rs2, rsend, rrec,
     local_sem, plus_s, plus_r, minus_s, minus_r, sib_s, sib_r, sent, p_r, d_r, ag1_r, ag2_r, ag2_rest, r1_r, r1_rest,
@@ -101,7 +102,7 @@
     moves = (
         (tok_hbm, tok_ref), (ids_hbm, ids_ref), (wts_hbm, wts_ref), (ngain_hbm, ngain_ref), (spread_hbm, spread_ref),
         (q_hbm, q_ref), (k_hbm, kv.at[ep, 0]), (v_hbm, kv.at[ep, 1]), (pack_hbm, pack_ref), (unpack_hbm, unpack_ref),
-        (lam_hbm, lam_ref), (gain_hbm, gain_ref),
+        (gain_hbm, gain_ref),
         (gate_hbm, gate_ref), (up_hbm, up_ref), (down_hbm, down_ref), (ow_hbm, ow_ref),
     )
     local = [pltpu.make_async_copy(src, dst, local_sem.at[i]) for i, (src, dst) in enumerate(moves)]
@@ -283,7 +284,7 @@
 
     def attend_close():
         ratio = acc_ref[...] / l_ref[...]
-        attended = ratio[:TOK] - lam_ref[...] * ratio[TOK:]
+        attended = ratio[:TOK] - lam_ref[0] * ratio[TOK:]
         square = jnp.mean(attended * attended, axis=-1, keepdims=True)
         head = (attended * lax.rsqrt(square + NORM_EPS) * gain_ref[...]).astype(BF16)
         product = mm(head, ow_ref[...])
@@ -314,6 +315,11 @@
             for j in far_first:
                 share_second(h, j).start()
 
+    first_at = (x, y)
+    second_at = (y, x)
+    own_block = (tp, x * SIDE + y)
+    turned = [(n % SIDE) * SIDE + n // SIDE for n in range(TP)]
+
     def rows(k, h):
         return pl.ds(pl.multiple_of(chunk[k] * TILE + h * HALF, HALF), HALF)
 
@@ -321,11 +327,9 @@
         return pl.ds(pl.multiple_of(chunk[k] * TILE, TILE), TILE)
 
     def ag1(k, h, j):
-        part = xall.at[rows(k, h), lanes(tp)]
+        part = xall.at[rows(k, h), lanes(own_block[h])]
         return remote(part, part, sent.at[1], ag1_r.at[k], ep, x_peer(j) if h == 0 else y_peer(j))
 
-    second_at = (y, x)
-    first_at = (x, y)
 
     def along(h, j):
         return y_peer(j) if h == 0 else x_peer(j)
@@ -333,14 +337,8 @@
     def across(h, j):
         return x_peer(j) if h == 0 else y_peer(j)
 
-    def columns(h, q, half):
-        q = q % SIDE
-        if h == 0:
-            return [lanes(2 * q + half, PAIR)]
-        return [lanes((2 * half + i) * SIDE + q) for i in range(2)]
-
-    def pieces(h):
-        return range(1 + h)
+    def columns(q, half):
+        return lanes(2 * (q % SIDE) + half, PAIR)
 
     def ahead(s):
         return 1 if s == 0 else SIDE - 1
@@ -348,27 +346,26 @@
     def behind(s):
         return SIDE - ahead(s)
 
-    def ag2(k, h, s, half, i, q):
-        part = xall.at[rows(k, h), columns(h, q, half)[i]]
+    def ag2(k, h, s, half, q):
+        part = xall.at[rows(k, h), columns(q, half)]
         sem = ag2_r.at[k, h, s] if half == s else ag2_rest.at[k]
         return remote(part, part, sent.at[2], sem, ep, along(h, ahead(s)))
 
-    def ag2_relay(k, h, s, i, q):
-        part = xall.at[rows(k, h), columns(h, q, s)[i]]
+    def ag2_relay(k, h, s, q):
+        part = xall.at[rows(k, h), columns(q, s)]
         return remote(part, part, sent.at[2], ag2_rest.at[k], ep, along(h, ahead(s)))
 
-    def rs1_raw(k, h, s, kind, i):
+    def rs1_raw(k, h, s, kind):
         q, half = (second_at[h] + 2, s) if kind == 0 else (second_at[h] + ahead(s), 1 - s)
-        part = ypart.at[rows(k, h), columns(h, q, half)[i]]
-        to = rs1.at[k, h, kind, s] if h == 0 else rs1.at[k, h, kind, s, :, pl.ds(i * LANE, LANE)]
+        part = ypart.at[rows(k, h), columns(q, half)]
         sem = r1_r.at[k, h, s] if kind == 0 else r1_rest.at[k, h]
-        return remote(part, to, sent.at[3], sem, ep, along(h, ahead(s)))
+        return remote(part, rs1.at[k, h, kind, s], sent.at[3], sem, ep, along(h, ahead(s)))
 
     def rs1_comb(k, h, s):
         return remote(comb.at[k, h, s], rs1.at[k, h, 2, s], sent.at[3], r1_rest.at[k, h], ep, along(h, ahead(s)))
 
     def share_of(k, h, q, half):
-        return jnp.concatenate([ypart[rows(k, h), c].astype(F32) for c in columns(h, q, half)], axis=1)
+        return ypart[rows(k, h), columns(q, half)].astype(F32)
 
     def rs2_copy(k, h, j):
         part = band.at[k, h, :, lanes((first_at[h] + j) % SIDE)]
@@ -381,7 +378,9 @@
     def gather_open(k):
         arrived(xrec.at[pl.ds(chunk[k] * SOURCES, len(others(k)))], d_r.at[chunk[k]])
         got = jnp.concatenate([xrec[chunk[k] * SOURCES + s] for s in range(SOURCES)], axis=0)
-        xall[all_rows(k), lanes(tp)] = mm(pack_ref[...], got).astype(BF16)
+        packed = mm(pack_ref[...], got).astype(BF16)
+        for h in range(2):
+            xall[rows(k, h), lanes(own_block[h])] = packed[h * HALF : (h + 1) * HALF]
         for j in far_first:
             for h in range(2):
                 ag1(k, h, j).start()
@@ -391,28 +390,29 @@
         for turn in range(2):
             for h in range(2):
                 for s in range(2):
-                    for i in pieces(h):
-                        ag2(k, h, s, (s + turn) % 2, i, second_at[h]).start()
+                    ag2(k, h, s, (s + turn) % 2, second_at[h]).start()
 
     def gather_relay(k):
         for h in range(2):
             for s in range(2):
                 arrived(xall.at[rows(k, h), pl.ds(0, PAIR)], ag2_r.at[k, h, s])
-                for i in pieces(h):
-                    ag2_relay(k, h, s, i, second_at[h] + behind(s)).start()
+                ag2_relay(k, h, s, second_at[h] + behind(s)).start()
 
     def experts(k):
         arrived(xall.at[all_rows(k), pl.ds(0, 4 * PAIR)], ag2_rest.at[k])
-        block = xall[all_rows(k), :]
+        lower = jnp.concatenate([xall[rows(k, 1), n * LANE : (n + 1) * LANE] for n in turned], axis=1)
+        block = jnp.concatenate([xall[rows(k, 0), :], lower], axis=0)
         gated = jnp.minimum(mm(block, gate_ref[...]), CLAMP_LIMIT)
         clipped = jnp.clip(mm(block, up_ref[...]), -CLAMP_LIMIT, CLAMP_LIMIT)
         active = ((clipped + 1.0) * gated * jax.nn.sigmoid(GATE_SLOPE * gated)).astype(BF16)
-        ypart[all_rows(k), :] = mm(active, down_ref[...]).astype(BF16)
+        result = mm(active, down_ref[...]).astype(BF16)
+        ypart[rows(k, 0), :] = result[:HALF]
+        for n in range(TP):
+            ypart[rows(k, 1), turned[n] * LANE : (turned[n] + 1) * LANE] = result[HALF:, n * LANE : (n + 1) * LANE]
         for kind in range(2):
             for h in range(2):
                 for s in range(2):
-                    for i in pieces(h):
-                        rs1_raw(k, h, s, kind, i).start()
+                    rs1_raw(k, h, s, kind).start()
 
     def sum_relay(k):
         for h in range(2):
@@ -482,13 +482,14 @@
     sum_relay(1)
     attend_plus(3)
     experts(3)
+    sum_relay(2)
+    pl.when(z < EARLY)(attend_close)
     ring_step(7)
     attend_minus(3)
     sum_open(1)
-    sum_relay(2)
     sum_close(0)
+    sum_relay(3)
     ring_step(8)
-    sum_relay(3)
     attend_plus(5)
     attend_minus(5)
     sum_open(2)
@@ -496,8 +497,9 @@
     attend_plus(7)
     attend_last()
     sum_open(3)
-    attend_close()
+    pl.when(z >= EARLY)(attend_close)
     sum_close(2)
+    pl.when(z < EARLY)(share_sum)
 
     places = jnp.transpose(place).astype(BF16)
     slots = jnp.abs(mm(places, spread_ref[...], NT)) < 0.5
@@ -509,7 +511,7 @@
         parts.append(jnp.where(slots, mm(part, spread_ref[...], NT), 0.0).astype(BF16))
 
     sum_close(3)
-    share_sum()
+    pl.when(z >= EARLY)(share_sum)
 
     left(xsend.at[pl.ds(0, EP - 1)], 0)
     left(xall.at[pl.ds(0, TILE), pl.ds(0, 12 * LANE)], 1)
@@ -560,11 +562,10 @@
         kernel,
         name="layer",
         out_shape=(jax.ShapeDtypeStruct((TOK // TP, D), BF16), jax.ShapeDtypeStruct((TOK, LANE), BF16)),
-        in_specs=[hbm] * 16,
+        in_specs=[hbm] * 3 + [pl.BlockSpec(memory_space=pltpu.SMEM)] + [hbm] * 12,
         out_specs=(vmem, vmem),
         scratch_shapes=[
             pltpu.VMEM((TOK, LANE), BF16),
-            pltpu.VMEM((1, 1), F32),
             pltpu.VMEM((1, LANE), F32),
             pltpu.VMEM((LANE, D), BF16),
             pltpu.VMEM((TOK, D), BF16),
@@ -595,7 +596,7 @@
             pltpu.VMEM((STEPS, 2, SIDE - 1, HALF, LANE), BF16),
             pltpu.VMEM((EP, SLAB, LANE), BF16),
             pltpu.VMEM((EP, SLAB, LANE), BF16),
-            dma((16,)),
+            dma((15,)),
             dma((8,)), dma((9,)), dma((7,)), dma((8,)), dma((CHIPS,)), dma((CHIPS,)),
             dma((8,)), dma((2,)), dma((STEPS,)), dma((STEPS,)), dma((STEPS, 2, 2)), dma((STEPS,)), dma((STEPS, 2, 2)),
             dma((STEPS, 2)), dma((STEPS,)), dma((1,)),
@@ -605,7 +606,7 @@
         ),
     )(
         query_maps.reshape(TOK, LANE), key_maps.reshape(TOK, LANE), value_rows.reshape(TOK, LANE),
-        head_lambda.reshape(1, 1), head_gain.reshape(1, LANE), out_weight, token_rows, norm_gain.reshape(1, D),
+        head_lambda, head_gain.reshape(1, LANE), out_weight, token_rows, norm_gain.reshape(1, D),
         expert_ids.T, route_weights.T, spread, pack, unpack,
         gate_weight.reshape(D, UNITS), up_weight.reshape(D, UNITS), down_weight.reshape(UNITS, D),
     )

time: 72.7 us -> 72.2 us (level)
  no operation moved by 1% of the time
where the time goes in v4:
time: 72.2 us; the launch traced here: 71.6 us
  Pallas kernels  68.3 us (95%)
  local copies, waits for them, and re-layouts  2 us (3%)
  between operations  1.3 us (2%)
    pallas_call x1, Pallas kernels, body(): pl.pallas_call(kernel, name='layer', out_shape=(jax.ShapeDtypeStruct((TOK...  68.3 us
    unnamed x4, local copies, waits for them, and re-layouts  2 us

profile of v4, /device:TPU:1, one launch (start us, length us, event | category | flops | bytes accessed | tf_op | source)
XLA Modules:
  0.0 71.6 jit_solution(1726427866474548997)
XLA Ops:
  1.3 68.3 %layer.1 = (bf16[8,2048]{1,0:T(8,128)(2,1)}, bf16[128,128]{1,0:T(8,128)(2,1)}) custom-call(bf16[128,128]{1,0:T(8,128)(2,1)} %bitcast.13, bf16[128,128]{1,0:T(8,128)(2,1)} %bitcast.14, bf16[128,128]{1,0:T(8,128)(2,1)} %bitcast.15, f32[1]{0:T(128)S(6)} %copy.20.lam_ref, f32[1,128]{1,0:T(1,128)} %bitcast.19, bf16[128,2048]{1,0:T(8,128)(2,1)} %ow_hbm.1, ...), custom_call_target="tpu_custom_call" | custom-call | tf_op jit(solution)/shard_map/layer/pallas_call | solution.py:561
  69.6 0.0 copy-start
  69.6 1.4 %copy.21 = bf16[8,2048]{1,0:T(8,128)(2,1)} copy(bf16[8,2048]{1,0:T(8,128)(2,1)} %get-tuple-element.4) | data formatting | bytes 65536
  71.0 0.0 copy-done
  71.0 0.6 copy.22
Async XLA Ops:
  69.6 1.4 %copy-start = (bf16[128,128]{1,0:T(8,128)(2,1)S(1)}, bf16[128,128]{1,0:T(8,128)(2,1)}, u32[]{:S(2)}) copy-start(bf16[128,128]{1,0:T(8,128)(2,1)} %get-tuple-element.5) | copy-start | bytes 98308

commit v5 on v4

--- a/solution.py
+++ b/solution.py
@@ -14,7 +14,7 @@
 MESH = pl.DeviceIdType.MESH
 
 EP, TP, SIDE, CHIPS = 32, 16, 4, 16
-CAP, SLAB = 20, 24
+CAP, SLAB = 20, 20
 ORDER = ((0, 1, 2, 3), (1, 0, 3, 2), (2, 0, 1, 3), (3, 0, 1, 2))
 OUTWARD = ((0, 2, 1, 3), (1, 0, 2, 3), (2, 0, 1, 3), (3, 1, 0, 2))
 STEPS = len(ORDER)
@@ -42,17 +42,14 @@
     spread = np.zeros((PADDED, LANE), np.float32)
     spread[rows, rows // SLAB] = 1.0
     spread[rows, EP] = -(rows % SLAB)
-    pack = np.zeros((TILE, PADDED_TILE), np.float32)
-    r = np.arange(TILE)
-    pack[r, r // CAP * SLAB + r % CAP] = 1.0
-    return spread, pack, pack.T.copy()
+    return spread
 
 
 def kernel(
-    q_hbm, k_hbm, v_hbm, lam_ref, gain_hbm, ow_hbm, tok_hbm, ngain_hbm, ids_hbm, wts_hbm, spread_hbm, pack_hbm,
-    unpack_hbm, gate_hbm, up_hbm, down_hbm,
+    q_hbm, k_hbm, v_hbm, lam_ref, gain_hbm, ow_hbm, tok_hbm, ngain_hbm, ids_hbm, wts_hbm, spread_hbm,
+    gate_hbm, up_hbm, down_hbm,
     rows_ref, experts_ref,
-    q_ref, gain_ref, ow_ref, tok_ref, ngain_ref, ids_ref, wts_ref, spread_ref, pack_ref, unpack_ref,
+    q_ref, gain_ref, ow_ref, tok_ref, ngain_ref, ids_ref, wts_ref, spread_ref,
     gate_ref, up_ref, down_ref,
     kv, m_ref, l_ref, acc_ref, ps, pa, pb, pc, xsend, xrec, xall, ypart, rs1, comb, band, rs2, rsend, rrec,
     local_sem, plus_s, plus_r, minus_s, minus_r, sib_s, sib_r, sent, p_r, d_r, ag1_r, ag2_r, ag2_rest, r1_r, r1_rest,
@@ -101,7 +98,7 @@
 
     moves = (
         (tok_hbm, tok_ref), (ids_hbm, ids_ref), (wts_hbm, wts_ref), (ngain_hbm, ngain_ref), (spread_hbm, spread_ref),
-        (q_hbm, q_ref), (k_hbm, kv.at[ep, 0]), (v_hbm, kv.at[ep, 1]), (pack_hbm, pack_ref), (unpack_hbm, unpack_ref),
+        (q_hbm, q_ref), (k_hbm, kv.at[ep, 0]), (v_hbm, kv.at[ep, 1]),
         (gain_hbm, gain_ref),
         (gate_hbm, gate_ref), (up_hbm, up_ref), (down_hbm, down_ref), (ow_hbm, ow_ref),
     )
@@ -378,9 +375,8 @@
     def gather_open(k):
         arrived(xrec.at[pl.ds(chunk[k] * SOURCES, len(others(k)))], d_r.at[chunk[k]])
         got = jnp.concatenate([xrec[chunk[k] * SOURCES + s] for s in range(SOURCES)], axis=0)
-        packed = mm(pack_ref[...], got).astype(BF16)
         for h in range(2):
-            xall[rows(k, h), lanes(own_block[h])] = packed[h * HALF : (h + 1) * HALF]
+            xall[rows(k, h), lanes(own_block[h])] = got[h * HALF : (h + 1) * HALF]
         for j in far_first:
             for h in range(2):
                 ag1(k, h, j).start()
@@ -440,10 +436,9 @@
             for j in (1, 2, 3):
                 total = total + rs2[k, h, j - 1].astype(F32)
             halves.append(total)
-        total = jnp.concatenate(halves, axis=0).astype(BF16)
-        result = mm(unpack_ref[...], total).astype(BF16)
+        total = jnp.concatenate(halves, axis=0)
         for s in range(SOURCES):
-            rsend[chunk[k] * SOURCES + s] = result[s * SLAB : (s + 1) * SLAB]
+            rsend[chunk[k] * SOURCES + s] = total[s * SLAB : (s + 1) * SLAB].astype(BF16)
         for i in others(k):
             give_back(k, i).start()
         if k == 0:
@@ -554,7 +549,7 @@
     query_maps, key_maps, value_rows, head_lambda, head_gain, out_weight, token_rows, norm_gain, expert_ids,
     route_weights, gate_weight, up_weight, down_weight,
 ):
-    spread, pack, unpack = (jnp.asarray(a, BF16) for a in slot_tables())
+    spread = jnp.asarray(slot_tables(), BF16)
     vmem = pl.BlockSpec(memory_space=pltpu.VMEM)
     hbm = pl.BlockSpec(memory_space=pl.ANY)
     dma = pltpu.SemaphoreType.DMA
@@ -562,7 +557,7 @@
         kernel,
         name="layer",
         out_shape=(jax.ShapeDtypeStruct((TOK // TP, D), BF16), jax.ShapeDtypeStruct((TOK, LANE), BF16)),
-        in_specs=[hbm] * 3 + [pl.BlockSpec(memory_space=pltpu.SMEM)] + [hbm] * 12,
+        in_specs=[hbm] * 3 + [pl.BlockSpec(memory_space=pltpu.SMEM)] + [hbm] * 10,
         out_specs=(vmem, vmem),
         scratch_shapes=[
             pltpu.VMEM((TOK, LANE), BF16),
@@ -573,8 +568,6 @@
             pltpu.VMEM((4, TOK), jnp.int32),
             pltpu.VMEM((4, TOK), F32),
             pltpu.VMEM((PADDED, LANE), BF16),
-            pltpu.VMEM((TILE, PADDED_TILE), BF16),
-            pltpu.VMEM((PADDED_TILE, TILE), BF16),
             pltpu.VMEM((D, UNITS), BF16),
             pltpu.VMEM((D, UNITS), BF16),
             pltpu.VMEM((UNITS, D), BF16),
@@ -596,7 +589,7 @@
             pltpu.VMEM((STEPS, 2, SIDE - 1, HALF, LANE), BF16),
             pltpu.VMEM((EP, SLAB, LANE), BF16),
             pltpu.VMEM((EP, SLAB, LANE), BF16),
-            dma((15,)),
+            dma((13,)),
             dma((8,)), dma((9,)), dma((7,)), dma((8,)), dma((CHIPS,)), dma((CHIPS,)),
             dma((8,)), dma((2,)), dma((STEPS,)), dma((STEPS,)), dma((STEPS, 2, 2)), dma((STEPS,)), dma((STEPS, 2, 2)),
             dma((STEPS, 2)), dma((STEPS,)), dma((1,)),
@@ -607,7 +600,7 @@
     )(
         query_maps.reshape(TOK, LANE), key_maps.reshape(TOK, LANE), value_rows.reshape(TOK, LANE),
         head_lambda, head_gain.reshape(1, LANE), out_weight, token_rows, norm_gain.reshape(1, D),
-        expert_ids.T, route_weights.T, spread, pack, unpack,
+        expert_ids.T, route_weights.T, spread,
         gate_weight.reshape(D, UNITS), up_weight.reshape(D, UNITS), down_weight.reshape(UNITS, D),
     )
 

time: 72.2 us -> 71.9 us (level)
  no operation moved by 1% of the time
where the time goes in v5:
time: 71.9 us; the launch traced here: 71.3 us
  Pallas kernels  68 us (95%)
  local copies, waits for them, and re-layouts  2 us (3%)
  between operations  1.3 us (2%)
    pallas_call x1, Pallas kernels, body(): pl.pallas_call(kernel, name='layer', out_shape=(jax.ShapeDtypeStruct((TOK...  68 us
    unnamed x4, local copies, waits for them, and re-layouts  2 us

profile of v5, /device:TPU:1, one launch (start us, length us, event | category | flops | bytes accessed | tf_op | source)
XLA Modules:
  0.0 71.3 jit_solution(17199889389238956074)
XLA Ops:
  1.3 68.0 %layer.1 = (bf16[8,2048]{1,0:T(8,128)(2,1)}, bf16[128,128]{1,0:T(8,128)(2,1)}) custom-call(bf16[128,128]{1,0:T(8,128)(2,1)} %bitcast.13, bf16[128,128]{1,0:T(8,128)(2,1)} %bitcast.14, bf16[128,128]{1,0:T(8,128)(2,1)} %bitcast.15, f32[1]{0:T(128)S(6)} %copy.18.lam_ref, f32[1,128]{1,0:T(1,128)} %bitcast.19, bf16[128,2048]{1,0:T(8,128)(2,1)} %ow_hbm.1, ...), custom_call_target="tpu_custom_call" | custom-call | tf_op jit(solution)/shard_map/layer/pallas_call | solution.py:556
  69.2 0.0 copy-start
  69.3 1.4 %copy.19 = bf16[8,2048]{1,0:T(8,128)(2,1)} copy(bf16[8,2048]{1,0:T(8,128)(2,1)} %get-tuple-element.4) | data formatting | bytes 65536
  70.6 0.0 copy-done
  70.6 0.6 copy.20
Async XLA Ops:
  69.2 1.4 %copy-start = (bf16[128,128]{1,0:T(8,128)(2,1)S(1)}, bf16[128,128]{1,0:T(8,128)(2,1)}, u32[]{:S(2)}) copy-start(bf16[128,128]{1,0:T(8,128)(2,1)} %get-tuple-element.5) | copy-start | bytes 98308
